TPU v7x, 256 devices: a whole 4x4x8 slice. The times are simulated.
256 devices in a mesh: ep: 64 (over z, y, core), tp: 4 (over x).
Axes of the slice: x: 4, y: 4, z: 8, core: 2. Of those that a mesh axis runs over, the one named last changes fastest.
Arguments:
- tokens: bfloat16 [2048, 2048], P('ep', 'tp'), may hold values from -33 to 33
- previous: bfloat16 [2048, 2048], P('ep', 'tp'), may hold values from -6 to 6
- first_norm_gain: float32 [2048], replicated, may hold values from 0.1 to 1.9
- token_shift_share: float32 [5, 2048], replicated, may hold values from 0 to 1
- receptance_weight: bfloat16 [2048, 1024], P(None, 'tp'), may hold values from -0.125 to 0.125
- key_weight: bfloat16 [2048, 1024], P(None, 'tp'), may hold values from -0.125 to 0.125
- value_weight: bfloat16 [2048, 1024], P(None, 'tp'), may hold values from -0.125 to 0.125
- decay_down_map: bfloat16 [2048, 128], replicated, may hold values from -0.125 to 0.125
- decay_up_map: bfloat16 [128, 1024], replicated, may hold values from -0.5 to 0.5
- decay_offset: float32 [1024], P('tp'), may hold values from -4 to 1
- strength_down_map: bfloat16 [2048, 128], replicated, may hold values from -0.125 to 0.125
- strength_up_map: bfloat16 [128, 1024], replicated, may hold values from -0.5 to 0.5
- removal_key_scale: float32 [1024], P('tp'), may hold values from 0.3 to 3
- key_damping: float32 [1024], P('tp'), may hold values from 0.1 to 1.9
- self_term_weight: float32 [16, 64], P('tp'), may hold values from -0.6 to 0.6
- head_norm_gain: float32 [1024], P('tp'), may hold values from 0.1 to 1.9
- output_weight: bfloat16 [1024, 2048], P('tp'), may hold values from -0.1875 to 0.1875
- state: float32 [2048, 16, 64, 64], P('ep', 'tp'), may hold values from -6 to 6
- second_norm_gain: float32 [2048], replicated, may hold values from 0.1 to 1.9
- routes: int32 [2048, 4], P('ep'), may hold values from 0 to 63, all different within a row; in each aligned block of 32 rows (0 to 31, 32 to 63, ...) at most 3 rows name the same one
- chosen_expert_weight: float32 [2048, 4], P('ep'), may hold values from 0.1 to 1
- expert_gate_weight: bfloat16 [64, 2048, 1024], P('ep', None, 'tp'), may hold values from -0.5 to 0.5
- expert_up_weight: bfloat16 [64, 2048, 1024], P('ep', None, 'tp'), may hold values from -0.5 to 0.5
- expert_down_weight: bfloat16 [64, 1024, 2048], P('ep', 'tp'), may hold values from -0.046875 to 0.046875
Outputs:
- layer_out: bfloat16 [2048, 2048], P('ep', 'tp')
- new_state: float32 [2048, 16, 64, 64], P('ep', 'tp')
Inputs may be any that keep to these rules, and one draw needn't show every extreme that they name: `routes`: each row names 4 different experts. Among the rows of one index of ep no expert is named by more than 3 rows, and in every draw some expert is named by exactly 3 rows of some index of ep.
All inputs are finite; a program needn't handle non-finite values.
Results may differ from a plain program's by a relative error of at most 0.015.
Values may be sent and summed in bfloat16 or wider, within the bound.
A program may use at most 64 MiB of HBM per device.

v0:
```python
import jax
import jax.numpy as jnp
from jax import lax
from jax.sharding import PartitionSpec as P

NORM_EPS = 1e-06
GROUP_EPS = 0.00064
KEY_EPS = 1e-06
GATE_LIMIT = 7.0
GATE_SLOPE = 1.702


def in_one_piece(arrays, axis, dim, along):
    widths = [a.shape[along] for a in arrays]
    both = jnp.concatenate(arrays, axis=along)
    result = lax.all_gather(both, axis, axis=dim, tiled=True)
    return tuple(jnp.split(result, [sum(widths[:k]) for k in range(1, len(widths))], axis=along))


def sent_to_all(value, axis):
    devices = lax.axis_size(axis)
    return lax.all_to_all(
        jnp.broadcast_to(value[None], (devices, *value.shape)), axis, 0, 0, tiled=True
    )


def of_everyone(value, axis):
    return sent_to_all(value, axis).astype(jnp.float32).sum(axis=0)


def cut_along(value, dim, devices):
    shape = value.shape
    tiles = value.reshape(*shape[:dim], devices, shape[dim] // devices, *shape[dim + 1 :])
    return jnp.moveaxis(tiles, dim, 0)


def summed_on_arrival(value, axis, dim):
    tiles = cut_along(value, dim, lax.axis_size(axis))
    arrived = lax.all_to_all(tiles, axis, split_axis=0, concat_axis=0, tiled=True)
    return arrived.astype(jnp.float32).sum(axis=0)


def in_order(tiles, dim):
    tiles = jnp.moveaxis(tiles, 0, dim)
    shape = tiles.shape
    return tiles.reshape(*shape[:dim], shape[dim] * shape[dim + 1], *shape[dim + 2 :])


def gather_directly(value, axis, dim):
    tiles = sent_to_all(value, axis)
    return in_order(tiles, dim)


def row_rescale(values, gain):
    return values * lax.rsqrt(jnp.mean(values * values, axis=-1, keepdims=True) + NORM_EPS) * gain


def head_combiner(
    present_rows,
    prior_rows,
    first_norm_gain,
    token_shift_share,
    receptance_weight,
    key_weight,
    value_weight,
    decay_down_map,
    decay_up_map,
    decay_offset,
    strength_down_map,
    strength_up_map,
    removal_key_scale,
    key_damping,
    self_term_weight,
    head_norm_gain,
    state,
):
    sequence_count = present_rows.shape[0]
    head_number = state.shape[1]
    head_extent = state.shape[2]
    normed = row_rescale(present_rows.astype(jnp.float32), first_norm_gain)
    before = prior_rows.astype(jnp.float32)

    def shifted(role):
        return (normed + (before - normed) * token_shift_share[role]).astype(jnp.bfloat16)

    def project(inputs, weight):
        return jnp.dot(inputs, weight, preferred_element_type=jnp.float32)

    def by_heads(values):
        return values.reshape(sequence_count, head_number, head_extent)

    receptance_rows = by_heads(project(shifted(0), receptance_weight))
    key_rows = by_heads(project(shifted(1), key_weight))
    value_matrix = by_heads(project(shifted(2), value_weight))
    decay_low = jnp.tanh(project(shifted(3), decay_down_map)).astype(jnp.bfloat16)
    decay_pre = decay_offset + project(decay_low, decay_up_map)
    decay = by_heads(jnp.exp(-jnp.exp(-jax.nn.softplus(-decay_pre) - 0.5)))
    alpha_low = project(shifted(4), strength_down_map).astype(jnp.bfloat16)
    alpha = by_heads(jax.nn.sigmoid(project(alpha_low, strength_up_map)))
    removal = key_rows * removal_key_scale.reshape(head_number, head_extent)
    removal = removal * lax.rsqrt(jnp.sum(removal * removal, axis=-1, keepdims=True) + KEY_EPS)
    blended_rows = key_rows * (1.0 + (alpha - 1.0) * key_damping.reshape(head_number, head_extent))
    along = jnp.einsum("shij,shj->shi", state, removal)
    new_state = (
        state * decay[:, :, None, :]
        - along[..., None] * (removal * alpha)[:, :, None, :]
        + value_matrix[..., None] * blended_rows[:, :, None, :]
    )
    readout = jnp.einsum("shij,shj->shi", new_state, receptance_rows)
    centered = readout - jnp.mean(readout, axis=-1, keepdims=True)
    variance = jnp.mean(centered * centered, axis=-1, keepdims=True)
    heads_normalised = (
        centered
        * lax.rsqrt(variance + GROUP_EPS)
        * head_norm_gain.reshape(head_number, head_extent)
    )
    self_term = (
        jnp.sum(receptance_rows * blended_rows * self_term_weight, axis=-1, keepdims=True)
        * value_matrix
    )
    mixed_inputs = (
        (heads_normalised + self_term)
        .reshape(sequence_count, head_number * head_extent)
        .astype(jnp.bfloat16)
    )
    return (mixed_inputs, new_state)


def shards(
    tokens,
    previous,
    first_norm_gain,
    token_shift_share,
    receptance_weight,
    key_weight,
    value_weight,
    decay_down_map,
    decay_up_map,
    decay_offset,
    strength_down_map,
    strength_up_map,
    removal_key_scale,
    key_damping,
    self_term_weight,
    head_norm_gain,
    output_weight,
    state,
    second_norm_gain,
    routes,
    chosen_expert_weight,
    expert_gate_weight,
    expert_up_weight,
    expert_down_weight,
):
    present_rows, prior_rows = in_one_piece((tokens, previous), "tp", 1, 0)
    head_columns = receptance_weight.shape[1]
    head_start = lax.axis_index("tp") * head_columns
    decay_own = lax.dynamic_slice_in_dim(decay_up_map, head_start, head_columns, 1)
    alpha_own = lax.dynamic_slice_in_dim(strength_up_map, head_start, head_columns, 1)
    mixed_inputs, new_state = head_combiner(
        present_rows,
        prior_rows,
        first_norm_gain,
        token_shift_share,
        receptance_weight,
        key_weight,
        value_weight,
        decay_down_map,
        decay_own,
        decay_offset,
        strength_down_map,
        alpha_own,
        removal_key_scale,
        key_damping,
        self_term_weight,
        head_norm_gain,
        state,
    )
    head_terms = jnp.dot(mixed_inputs, output_weight, preferred_element_type=jnp.float32)
    own_columns = tokens.shape[1]
    column_start = lax.axis_index("tp") * own_columns
    residual = present_rows.astype(jnp.float32) + of_everyone(
        head_terms.astype(jnp.bfloat16), "tp"
    ).astype(jnp.float32)
    expert_rows = row_rescale(residual, second_norm_gain).astype(jnp.bfloat16)
    residual_own = lax.dynamic_slice_in_dim(residual, column_start, own_columns, 1)
    normed_own = lax.dynamic_slice_in_dim(expert_rows, column_start, own_columns, 1)
    sequences, choices_per = routes.shape
    experts = expert_gate_weight.shape[0] * lax.axis_size("ep")
    capacity = max(2, 3 * sequences * choices_per // (2 * experts))
    flattened = routes.reshape(-1)
    onehot = (flattened[:, None] == jnp.arange(experts, dtype=jnp.int32)[None, :]).astype(jnp.int32)
    ranking = jnp.sum((jnp.cumsum(onehot, axis=0) - onehot) * onehot, axis=1)
    slot_index = flattened * capacity + ranking
    placing = jnp.arange(experts * capacity, dtype=jnp.int32)[:, None] == slot_index[None, :]
    dispatch = jnp.sum(
        placing.reshape(experts * capacity, sequences, choices_per).astype(jnp.int32), axis=2
    ).astype(jnp.bfloat16)
    outgoing = jnp.dot(dispatch, normed_own, preferred_element_type=jnp.float32).astype(
        jnp.bfloat16
    )
    outgoing = outgoing.reshape(experts, capacity, -1)
    arrived = gather_directly(
        lax.all_to_all(outgoing, "ep", split_axis=0, concat_axis=0, tiled=True), "tp", 2
    )
    sources, slot_count, feature_count = arrived.shape
    expert_input = arrived.reshape(sources * slot_count, feature_count)
    gate_pre = jnp.minimum(
        jnp.dot(expert_input, expert_gate_weight[0], preferred_element_type=jnp.float32), GATE_LIMIT
    )
    up_pre = jnp.clip(
        jnp.dot(expert_input, expert_up_weight[0], preferred_element_type=jnp.float32),
        -GATE_LIMIT,
        GATE_LIMIT,
    )
    activation = ((up_pre + 1.0) * gate_pre * jax.nn.sigmoid(GATE_SLOPE * gate_pre)).astype(
        jnp.bfloat16
    )
    down_terms = jnp.dot(activation, expert_down_weight[0], preferred_element_type=jnp.float32)
    down_terms = down_terms.reshape(sources, slot_count, -1)
    shares = summed_on_arrival(down_terms.astype(jnp.bfloat16), "tp", 2).astype(jnp.bfloat16)
    returned = lax.all_to_all(shares, "ep", split_axis=0, concat_axis=0, tiled=True)
    returned_rows = returned.reshape(experts * capacity, -1)
    picked = jnp.take(returned_rows, slot_index, axis=0).astype(jnp.float32)
    weighted = jnp.sum(
        picked.reshape(sequences, choices_per, -1) * chosen_expert_weight[:, :, None], axis=1
    )
    layer_out = (residual_own + weighted).astype(jnp.bfloat16)
    return (layer_out, new_state)


def solution(mesh):
    in_specs = (
        P("ep", "tp"),
        P("ep", "tp"),
        P(),
        P(),
        P(None, "tp"),
        P(None, "tp"),
        P(None, "tp"),
        P(),
        P(),
        P("tp"),
        P(),
        P(),
        P("tp"),
        P("tp"),
        P("tp", None),
        P("tp"),
        P("tp", None),
        P("ep", "tp", None, None),
        P(),
        P("ep", None),
        P("ep", None),
        P("ep", None, "tp"),
        P("ep", None, "tp"),
        P("ep", "tp", None),
    )
    out_specs = (P("ep", "tp"), P("ep", "tp", None, None))
    return jax.shard_map(shards, mesh=mesh, in_specs=in_specs, out_specs=out_specs, check_vma=False)
```

profile of v0, /device:TPU:1, one launch (start us, length us, event | category | flops | bytes accessed | tf_op | source)
XLA Modules:
  0.0 125.7 jit_solution(13619742929195453664)
XLA Ops:
  0.7 0.9 pad_maximum_fusion
  1.6 11.0 %all_gather.3 = bf16[64,2048]{1,0:T(8,128)(2,1)S(1)} all-gather(bf16[64,512]{1,0:T(8,128)(2,1)S(1)} %pad_maximum_fusion), channel_id=1, replica_groups=mesh['ep'=64,'tp'=4] {'tp'}, dimensions={1}, use_global_device_ids=true | all-gather | bytes 327680 | tf_op jit(solution)/shard_map/all_gather | solution.py:16
  12.8 1.1 fusion.98
  13.8 1.6 %fusion.29 = f32[32,256]{1,0:T(8,128)S(1)} fusion(bf16[2048,256]{1,0:T(8,128)(2,1)} %param.28, f32[2048]{0:T(1024)S(1)} %bitcast.67, f32[2048]{0:T(1024)} %param.26, f32[32]{0:T(128)S(1)} %add_rsqrt_fusion.3, bf16[64,2048]{1,0:T(8,128)(2,1)S(1)} %all_gather.3), kind=kOutput, calls=%fused_computation.47 | convolution fusion | flops 34078720 | bytes 1360000 | tf_op jit(solution)/shard_map/dot_general | solution.py:87
  15.6 1.4 %fusion.10 = f32[32,256]{1,0:T(8,128)S(1)} fusion(bf16[2048,128]{1,0:T(8,128)(2,1)} %param.34, f32[2048]{0:T(1024)S(1)} %bitcast.69, f32[2048]{0:T(1024)} %param.26, f32[32]{0:T(128)S(1)} %add_rsqrt_fusion.3, bf16[64,2048]{1,0:T(8,128)(2,1)S(1)} %all_gather.3, bf16[128,1024]{1,0:T(8,128)(2,1)} %param.35, s32[]{:T(128)S(6)} %select_n.34), kind=kOutput, calls=%fused_computation.18 | convolution fusion | flops 19427328 | bytes 901252 | tf_op jit(solution)/shard_map/dot_general | solution.py:87
  17.1 1.6 %fusion.35 = f32[32,256]{1,0:T(8,128)S(1)} fusion(bf16[2048,256]{1,0:T(8,128)(2,1)} %param.29, f32[2048]{0:T(1024)S(1)} %bitcast.66, f32[2048]{0:T(1024)} %param.26, f32[32]{0:T(128)S(1)} %add_rsqrt_fusion.3, bf16[64,2048]{1,0:T(8,128)(2,1)S(1)} %all_gather.3), kind=kOutput, calls=%fused_computation.49 | convolution fusion | flops 34078720 | bytes 1360000 | tf_op jit(solution)/shard_map/dot_general | solution.py:87
  19.1 1.3 %fusion.82 = f32[32,256]{1,0:T(8,128)S(1)} fusion(bf16[128,1024]{1,0:T(8,128)(2,1)} %param.32, s32[]{:T(128)S(6)} %select_n.34, bf16[2048,128]{1,0:T(8,128)(2,1)S(1)} %copy-done.13, f32[2048]{0:T(1024)S(1)} %bitcast.68, f32[2048]{0:T(1024)S(1)} %copy-done.6, f32[32]{0:T(128)S(1)} %add_rsqrt_fusion.3, bf16[64,2048]{1,0:T(8,128)(2,1)S(1)} %all_gather.3, ...), kind=kOutput, calls=%fused_computation.96 | convolution fusion | flops 19492864 | bytes 902276 | tf_op jit(solution)/shard_map/dot_general | solution.py:87
  21.1 3.5 %fusion.99 = f32[32,4,1,64]{3,2,1,0:T(1,128)S(1)} fusion(f32[32,4,64,1]{2,3,1,0:T(1,128)S(1)} %bitcast.64, f32[32,4,64,64]{3,2,1,0:T(8,128)} %param.41), kind=kOutput, calls=%fused_computation.119 | convolution fusion | flops 1048576 | bytes 2162688 | tf_op jit(solution)/shard_map/shij,shj->shi/dot_general | solution.py:103
  24.6 2.8 %multiply_add_fusion = f32[32,4,64,64]{3,2,1,0:T(8,128)S(1)} fusion(f32[32,4,64,64]{3,2,1,0:T(8,128)S(1)} %copy-done.1, f32[32,4,64]{2,1,0:T(4,128)S(1)} %get-tuple-element.8, f32[32,4,64]{2,1,0:T(4,128)S(1)} %mul.306, f32[32,4,64]{2,1,0:T(4,128)S(1)} %get-tuple-element.6, f32[32,4,64]{2,1,0:T(4,128)S(1)} %bitcast.62, f32[32,4,64]{2,1,0:T(4,128)S(1)} %mul.284), kind=kLoop, calls=%fused_computation.2 | loop fusion | flops 2621440 | bytes 4358144 | tf_op jit(solution)/shard_map/add | solution.py:105
  27.5 2.0 %copy-done.2 = f32[32,4,64,64]{3,2,1,0:T(8,128)} copy-done((f32[32,4,64,64]{3,2,1,0:T(8,128)}, f32[32,4,64,64]{3,2,1,0:T(8,128)S(1)}, u32[]{:S(2)}) %copy-start.2) | copy-done | bytes 2097176
  29.4 1.2 fusion.100
  32.0 0.8 broadcast_in_dim.11
  32.8 3.5 %all-to-all-start = ((bf16[4,32,2048]{2,1,0:T(8,128)(2,1)}), bf16[4,32,2048]{2,1,0:T(8,128)(2,1)S(1)}, u32[]{:S(2)}, u32[]{:S(2)}) async-start(bf16[4,32,2048]{2,1,0:T(8,128)(2,1)} %broadcast_in_dim.11), calls=%async_computation | async-start | bytes 1048576 | tf_op jit(solution)/shard_map/all_to_all | solution.py:22
  37.1 0.8 dynamic-slice
  38.0 5.2 %all-to-all-done = bf16[4,32,2048]{2,1,0:T(8,128)(2,1)S(1)} async-done(((bf16[4,32,2048]{2,1,0:T(8,128)(2,1)}), bf16[4,32,2048]{2,1,0:T(8,128)(2,1)S(1)}, u32[]{:S(2)}, u32[]{:S(2)}) %all-to-all-start) | async-done | bytes 524320 | tf_op jit(solution)/shard_map/all_to_all | solution.py:22
  43.8 29.1 %all_to_all.25 = bf16[64,3,512]{2,1,0:T(4,128)(2,1)S(1)} all-to-all(bf16[64,3,512]{2,1,0:T(4,128)(2,1)S(1)} %reshape.165), channel_id=1, replica_groups=mesh['ep'=64,'tp'=4] {'ep'}, dimensions={0} | all-to-all | bytes 393216 | tf_op jit(solution)/shard_map/all_to_all | solution.py:204
  73.0 14.7 %all_to_all.26 = bf16[4,64,3,512]{3,1,2,0:T(8,128)(2,1)S(1)} all-to-all(bf16[4,64,3,512]{3,1,2,0:T(8,128)(2,1)S(1)} %broadcast_in_dim.13), channel_id=1, replica_groups=mesh['ep'=64,'tp'=4] {'tp'}, dimensions={0} | all-to-all | bytes 1572864 | tf_op jit(solution)/shard_map/all_to_all | solution.py:22
  87.7 0.6 copy.65
  89.8 13.7 %all_to_all.27 = bf16[4,64,3,512]{3,1,2,0:T(8,128)(2,1)S(1)} all-to-all(bf16[4,64,3,512]{3,1,2,0:T(8,128)(2,1)S(1)} %bitcast.55), channel_id=1, replica_groups=mesh['ep'=64,'tp'=4] {'tp'}, dimensions={0} | all-to-all | bytes 1572864 | tf_op jit(solution)/shard_map/all_to_all | solution.py:39
  103.7 0.9 copy.69
  104.5 6.1 %all-to-all-start.4 = ((bf16[64,3,512]{2,1,0:T(4,128)(2,1)}), bf16[64,3,512]{2,1,0:T(4,128)(2,1)S(1)}, u32[]{:S(2)}, u32[]{:S(2)}) async-start(bf16[64,3,512]{2,1,0:T(4,128)(2,1)} %copy.69), calls=%async_computation.4 | async-start | bytes 524288 | tf_op jit(solution)/shard_map/all_to_all | solution.py:222
  111.0 12.7 %all-to-all-done.4 = bf16[64,3,512]{2,1,0:T(4,128)(2,1)S(1)} async-done(((bf16[64,3,512]{2,1,0:T(4,128)(2,1)}), bf16[64,3,512]{2,1,0:T(4,128)(2,1)S(1)}, u32[]{:S(2)}, u32[]{:S(2)}) %all-to-all-start.4) | async-done | bytes 196640 | tf_op jit(solution)/shard_map/all_to_all | solution.py:222
  123.9 0.8 gather_fusion
  125.1 0.6 add_convert_fusion
  (86 shorter events, 6.9 us)
Async XLA Ops:
  0.6 88.7 %copy-start = (bf16[1,256,2048]{2,1,0:T(8,128)(2,1)S(1)}, bf16[1,256,2048]{2,1,0:T(8,128)(2,1)}, u32[]{:S(2)}) copy-start(bf16[1,256,2048]{2,1,0:T(8,128)(2,1)} %param.47) | copy-start | bytes 3145732
  0.6 18.5 %copy-start.6 = (f32[2048]{0:T(1024)S(1)}, f32[2048]{0:T(1024)}, u32[]{:S(2)}) copy-start(f32[2048]{0:T(1024)} %param.26) | copy-start | bytes 24580
  0.7 18.2 %copy-start.9 = (f32[256]{0:T(256)S(1)}, f32[256]{0:T(256)}, u32[]{:S(2)}) copy-start(f32[256]{0:T(256)} %param.36) | copy-start | bytes 3076
  0.7 18.4 %copy-start.10 = (f32[256]{0:T(256)S(1)}, f32[256]{0:T(256)}, u32[]{:S(2)}) copy-start(f32[256]{0:T(256)} %param.37) | copy-start | bytes 3076
  0.7 18.5 %copy-start.13 = (bf16[2048,128]{1,0:T(8,128)(2,1)S(1)}, bf16[2048,128]{1,0:T(8,128)(2,1)}, u32[]{:S(2)}) copy-start(bf16[2048,128]{1,0:T(8,128)(2,1)} %param.31) | copy-start | bytes 1572868
  0.7 18.4 %copy-start.15 = (f32[256]{0:T(256)S(1)}, f32[256]{0:T(256)}, u32[]{:S(2)}) copy-start(f32[256]{0:T(256)} %param.33) | copy-start | bytes 3076
  0.7 19.8 %copy-start.4 = (bf16[2048,256]{1,0:T(8,128)(2,1)S(1)}, bf16[2048,256]{1,0:T(8,128)(2,1)}, u32[]{:S(2)}) copy-start(bf16[2048,256]{1,0:T(8,128)(2,1)} %param.30) | copy-start | bytes 3145732
  21.0 3.6 %copy-start.1 = (f32[32,4,64,64]{3,2,1,0:T(8,128)S(1)}, f32[32,4,64,64]{3,2,1,0:T(8,128)}, u32[]{:S(2)}) copy-start(f32[32,4,64,64]{3,2,1,0:T(8,128)} %param.41) | copy-start | bytes 6291460
  27.4 2.0 %copy-start.2 = (f32[32,4,64,64]{3,2,1,0:T(8,128)}, f32[32,4,64,64]{3,2,1,0:T(8,128)S(1)}, u32[]{:S(2)}) copy-start(f32[32,4,64,64]{3,2,1,0:T(8,128)S(1)} %multiply_add_fusion) | copy-start | bytes 6291460
  27.4 3.5 %copy-start.11 = (f32[256]{0:T(256)S(1)}, f32[256]{0:T(256)}, u32[]{:S(2)}) copy-start(f32[256]{0:T(256)} %param.39) | copy-start | bytes 3076
  27.4 3.6 %copy-start.14 = (f32[4,64]{1,0:T(4,128)S(1)}, f32[4,64]{1,0:T(4,128)}, u32[]{:S(2)}) copy-start(f32[4,64]{1,0:T(4,128)} %param.38) | copy-start | bytes 3076
  27.5 4.2 %copy-start.3 = (bf16[256,2048]{1,0:T(8,128)(2,1)S(1)}, bf16[256,2048]{1,0:T(8,128)(2,1)}, u32[]{:S(2)}) copy-start(bf16[256,2048]{1,0:T(8,128)(2,1)} %param.40) | copy-start | bytes 3145732
  27.5 8.8 %copy-start.7 = (s32[32,4]{0,1:T(4,128)S(1)}, s32[32,4]{0,1:T(4,128)}, u32[]{:S(2)}) copy-start(s32[32,4]{0,1:T(4,128)} %param.43) | copy-start | bytes 1540
  32.8 10.4 %all-to-all-start = ((bf16[4,32,2048]{2,1,0:T(8,128)(2,1)}), bf16[4,32,2048]{2,1,0:T(8,128)(2,1)S(1)}, u32[]{:S(2)}, u32[]{:S(2)}) async-start(bf16[4,32,2048]{2,1,0:T(8,128)(2,1)} %broadcast_in_dim.11), calls=%async_computation | async-start | bytes 1048576 | tf_op jit(solution)/shard_map/all_to_all | solution.py:22
  43.3 45.2 %copy-start.5 = (bf16[1,2048,256]{2,1,0:T(8,128)(2,1)S(1)}, bf16[1,2048,256]{2,1,0:T(8,128)(2,1)}, u32[]{:S(2)}) copy-start(bf16[1,2048,256]{2,1,0:T(8,128)(2,1)} %param.45) | copy-start | bytes 3145732
  72.9 16.0 %copy-start.12 = (bf16[1,2048,256]{2,1,0:T(8,128)(2,1)S(1)}, bf16[1,2048,256]{2,1,0:T(8,128)(2,1)}, u32[]{:S(2)}) copy-start(bf16[1,2048,256]{2,1,0:T(8,128)(2,1)} %param.46) | copy-start | bytes 3145732
  89.3 21.6 %copy-start.8 = (f32[32,4]{0,1:T(4,128)S(1)}, f32[32,4]{0,1:T(4,128)}, u32[]{:S(2)}) copy-start(f32[32,4]{0,1:T(4,128)} %param.44) | copy-start | bytes 1540
  104.5 19.2 %all-to-all-start.4 = ((bf16[64,3,512]{2,1,0:T(4,128)(2,1)}), bf16[64,3,512]{2,1,0:T(4,128)(2,1)S(1)}, u32[]{:S(2)}, u32[]{:S(2)}) async-start(bf16[64,3,512]{2,1,0:T(4,128)(2,1)} %copy.69), calls=%async_computation.4 | async-start | bytes 524288 | tf_op jit(solution)/shard_map/all_to_all | solution.py:222
where the time goes:
time: 126 us
  blocking collectives  68.4 us (54%)
  waiting for transfers between devices  17.9 us (14%)
  matrix products  12.5 us (10%)
  starting transfers between devices  9.55 us (8%)
  local copies, waits for them, and re-layouts  9.45 us (7%)
  other arithmetic  6.78 us (5%)
    all_to_all x1, blocking collectives, shards(): lax.all_to_all(outgoing, 'ep', split_axis=0, concat_axis=0, tiled=True)  29.1 us
    all_to_all x1, blocking collectives, sent_to_all(): lax.all_to_all(jnp.broadcast_to(value[None], (devices, *value.shape)), ax...  14.7 us
    all_to_all x1, blocking collectives, summed_on_arrival(): lax.all_to_all(tiles, axis, split_axis=0, concat_axis=0, tiled=True)  13.7 us
    all_to_all x1, waiting for transfers between devices, shards(): lax.all_to_all(shares, 'ep', split_axis=0, concat_axis=0, tiled=True)  12.7 us
    all_gather x1, blocking collectives, in_one_piece(): result = lax.all_gather(both, axis, axis=dim, tiled=True)  11 us
    dot_general x5, matrix products, project(): return jnp.dot(inputs, weight, preferred_element_type=jnp.float32)  6.18 us
    all_to_all x1, starting transfers between devices, shards(): lax.all_to_all(shares, 'ep', split_axis=0, concat_axis=0, tiled=True)  6.08 us
    all_to_all x1, waiting for transfers between devices, sent_to_all(): lax.all_to_all(jnp.broadcast_to(value[None], (devices, *value.shape)), ax...  5.18 us
  transfers between devices with their start and end apart: 2, of which 2 were waited for; matrix products, arithmetic and copies ran while one was open for 2% of the time, Pallas kernels for 0%

commit v1 on v0

--- a/solution.py
+++ b/solution.py
@@ -1,6 +1,8 @@
 import jax
 import jax.numpy as jnp
 from jax import lax
+from jax.experimental import pallas as pl
+from jax.experimental.pallas import tpu as pltpu
 from jax.sharding import PartitionSpec as P
 
 NORM_EPS = 1e-06
@@ -15,40 +17,6 @@
     both = jnp.concatenate(arrays, axis=along)
     result = lax.all_gather(both, axis, axis=dim, tiled=True)
     return tuple(jnp.split(result, [sum(widths[:k]) for k in range(1, len(widths))], axis=along))
-
-
-def sent_to_all(value, axis):
-    devices = lax.axis_size(axis)
-    return lax.all_to_all(
-        jnp.broadcast_to(value[None], (devices, *value.shape)), axis, 0, 0, tiled=True
-    )
-
-
-def of_everyone(value, axis):
-    return sent_to_all(value, axis).astype(jnp.float32).sum(axis=0)
-
-
-def cut_along(value, dim, devices):
-    shape = value.shape
-    tiles = value.reshape(*shape[:dim], devices, shape[dim] // devices, *shape[dim + 1 :])
-    return jnp.moveaxis(tiles, dim, 0)
-
-
-def summed_on_arrival(value, axis, dim):
-    tiles = cut_along(value, dim, lax.axis_size(axis))
-    arrived = lax.all_to_all(tiles, axis, split_axis=0, concat_axis=0, tiled=True)
-    return arrived.astype(jnp.float32).sum(axis=0)
-
-
-def in_order(tiles, dim):
-    tiles = jnp.moveaxis(tiles, 0, dim)
-    shape = tiles.shape
-    return tiles.reshape(*shape[:dim], shape[dim] * shape[dim + 1], *shape[dim + 2 :])
-
-
-def gather_directly(value, axis, dim):
-    tiles = sent_to_all(value, axis)
-    return in_order(tiles, dim)
 
 
 def row_rescale(values, gain):
@@ -125,6 +93,309 @@
     )
     return (mixed_inputs, new_state)
 
+
+MESH = pl.DeviceIdType.MESH
+N_EP = 64
+N_TP = 4
+GROUPS = 4
+NS = N_EP // GROUPS
+ORDER = (0, 3, 1, 2)
+SLOTS = 3
+KEPT = 4 * SLOTS * NS
+PACKED = KEPT + NS
+F32 = jnp.float32
+BF16 = jnp.bfloat16
+
+
+def dot(a, b):
+    return jnp.dot(a, b, preferred_element_type=F32)
+
+
+def iota(shape, dim):
+    return lax.broadcasted_iota(jnp.int32, shape, dim)
+
+
+def third(m):
+    return (m * 11) >> 5
+
+
+def kept_row(m):
+    return jnp.where(m == 12, 3, m + third(m))
+
+
+def tail_kernel(
+    mixed_ref, tokens_ref, gain_ref, routes_ref, routes_row_ref, routes_tiled_ref, weight_ref,
+    wout_hbm, wg_hbm, wu_hbm, wd_hbm,
+    out_ref,
+    wout, wg, wu, wd, place, take, pick, unpick,
+    rs_send, rs_recv, residual, send_a, recv_a, gathered, down_send, down_recv, send_b, recv_b,
+    w_sem, rs_ssem, rs_rsem, a_ssem, a_rsem, g_ssem, g_rsem, d_ssem, d_rsem, b_ssem, b_rsem,
+):
+    me = lax.axis_index("ep")
+    tp = lax.axis_index("tp")
+    loads = [
+        pltpu.make_async_copy(wout_hbm, wout, w_sem.at[0]),
+        pltpu.make_async_copy(wg_hbm.at[0], wg, w_sem.at[1]),
+        pltpu.make_async_copy(wu_hbm.at[0], wu, w_sem.at[2]),
+        pltpu.make_async_copy(wd_hbm.at[0], wd, w_sem.at[3]),
+    ]
+    for load in loads:
+        load.start()
+    barrier = pltpu.get_barrier_semaphore()
+    for d in range(1, N_TP):
+        pl.semaphore_signal(
+            barrier, inc=1, device_id={"tp": lax.rem(tp + d, N_TP)}, device_id_type=MESH
+        )
+
+    def greet(d, carry):
+        pl.semaphore_signal(
+            barrier, inc=1, device_id={"ep": lax.rem(me + d, N_EP)}, device_id_type=MESH
+        )
+        return carry
+
+    lax.fori_loop(1, N_EP, greet, 0)
+
+    loads[0].wait()
+    for j in range(N_TP):
+        rs_send[j] = dot(mixed_ref[...], wout[:, j * 512 : (j + 1) * 512]).astype(BF16)
+    pl.semaphore_wait(barrier, N_EP - 1 + N_TP - 1)
+    rs_copies = []
+    for d in (2, 1, 3):
+        peer = lax.rem(tp + d, N_TP)
+        copy = pltpu.make_async_remote_copy(
+            src_ref=rs_send.at[peer], dst_ref=rs_recv.at[d - 1],
+            send_sem=rs_ssem.at[d - 1], recv_sem=rs_rsem.at[d - 1],
+            device_id={"tp": peer}, device_id_type=MESH,
+        )
+        copy.start()
+        rs_copies.append(copy)
+
+    lane = iota((1, 256), 1)
+    block, seq = lane // 32, lane % 32
+    source = iota((32, 256), 0)
+    targets = []
+    for c in range(4):
+        mine = routes_tiled_ref[c : c + 1, :]
+        rank = jnp.zeros((1, 256), jnp.int32)
+        for other in range(c + 1):
+            same = routes_ref[:, other : other + 1] == mine
+            if other == c:
+                same = same & (source < seq)
+            rank = rank + jnp.sum(same.astype(jnp.int32), axis=0, keepdims=True)
+        row = jnp.where(block < 4, block * 4 + rank, jnp.where(rank == block - 4, 3, -4096))
+        targets.append(mine * 16 + row)
+
+    def fill_place(i, carry):
+        at = pl.multiple_of(i * 128, 128)
+        row = iota((128, 256), 0) + at
+        hit = row == targets[0]
+        for c in range(1, 4):
+            hit = hit | (row == targets[c])
+        place[pl.ds(at, 128), :] = hit.astype(F32).astype(BF16)
+        return carry
+
+    lax.fori_loop(0, 8, fill_place, 0)
+
+    piece, tile_row = iota((PACKED, 16 * NS), 0), iota((PACKED, 16 * NS), 1)
+    pick[...] = (tile_row == (piece % NS) * 16 + kept_row(piece // NS)).astype(F32).astype(BF16)
+    tile_row, piece = iota((16 * NS, KEPT), 0), iota((16 * NS, KEPT), 1)
+    unpick[...] = (tile_row == (piece % NS) * 16 + kept_row(piece // NS)).astype(F32).astype(BF16)
+
+    for copy in rs_copies:
+        copy.wait()
+    total = tokens_ref[...].astype(F32) + rs_send[tp].astype(F32)
+    for d in range(N_TP - 1):
+        total = total + rs_recv[d].astype(F32)
+    residual[...] = total
+    square = jnp.sum(total * total, axis=1, keepdims=True)
+    high = square.astype(BF16).astype(F32)
+    low = square - high
+    scaled = total * gain_ref[pl.ds(tp, 1), :]
+    stack = [scaled[:, k * 128 : (k + 1) * 128] for k in range(4)]
+    sum_lane = iota((32, 128), 1)
+    for j in range(SLOTS):
+        stack.append(jnp.where(sum_lane == j, high, jnp.where(sum_lane == 3 + j, low, 0.0)))
+    stack.append(jnp.zeros((32, 128), F32))
+    stack = jnp.concatenate(stack, axis=0).astype(BF16)
+    send_a[...] = dot(place[...], stack).astype(BF16).reshape(N_EP, 16, 128)
+
+    def out_copy(r, group):
+        peer = lax.rem(me + N_EP - r, N_EP)
+        return pltpu.make_async_remote_copy(
+            src_ref=send_a.at[peer], dst_ref=recv_a.at[r],
+            send_sem=a_ssem, recv_sem=a_rsem.at[group],
+            device_id={"ep": peer}, device_id_type=MESH,
+        )
+
+    for group in ORDER:
+
+        def send_out(r, carry, group=group):
+            out_copy(r, group).start()
+            return carry
+
+        lax.fori_loop(max(1, group * NS), (group + 1) * NS, send_out, 0)
+    recv_a[0] = send_a[me]
+
+    seq_col = iota((32, 128), 0)
+    earlier = iota((32, 128), 1)
+    columns = []
+    for c in range(4):
+        mine = routes_ref[:, c : c + 1]
+        same = (routes_row_ref[...] == mine) & (earlier < c * 32 + seq_col)
+        columns.append(mine * 16 + jnp.sum(same.astype(jnp.int32), axis=1, keepdims=True))
+    for k in range(4):
+        for j in range(8):
+            at = iota((32, 128), 1) + (j * 128 - k * 4)
+            share = jnp.zeros((32, 128), F32)
+            for c in range(4):
+                share = jnp.where(at == columns[c], weight_ref[:, c : c + 1], share)
+            upper = share.astype(BF16)
+            take[k * 32 : (k + 1) * 32, j * 128 : (j + 1) * 128] = upper
+            take[128 + k * 32 : 160 + k * 32, j * 128 : (j + 1) * 128] = (
+                share - upper.astype(F32)
+            ).astype(BF16)
+
+    def wait_bytes(ref, sem):
+        pltpu.make_async_copy(ref, ref, sem).wait()
+
+    g_copies = []
+    for n, group in enumerate(ORDER):
+        first = group * NS
+        count = NS - 1 if group == 0 else NS
+        wait_bytes(recv_a.at[pl.ds(first, count)], a_rsem.at[group])
+        tiles = recv_a[first : first + NS].reshape(NS * 16, 128)
+        gathered[n, tp] = dot(pick[...], tiles).astype(BF16)
+        for d in (2, 1, 3):
+            copy = pltpu.make_async_remote_copy(
+                src_ref=gathered.at[n, tp], dst_ref=gathered.at[n, tp],
+                send_sem=g_ssem.at[n, d - 1], recv_sem=g_rsem.at[n, d - 1],
+                device_id={"tp": lax.rem(tp + d, N_TP)}, device_id_type=MESH,
+            )
+            copy.start()
+            g_copies.append(copy)
+    for load in loads[1:]:
+        load.wait()
+    d_copies = []
+    for n, group in enumerate(ORDER):
+        for copy in g_copies[3 * n : 3 * n + 3]:
+            copy.wait_recv()
+        rows, sums = [], None
+        for t in range(N_TP):
+            for k in range(4):
+                rows.append(gathered[n, t, k * 3 * NS : (k + 1) * 3 * NS, :])
+            part = gathered[n, t, KEPT:PACKED, :].astype(F32)
+            sums = part if sums is None else sums + part
+        rows = jnp.concatenate(rows, axis=1)
+        square = jnp.concatenate(
+            [sums[:, j : j + 1] + sums[:, 3 + j : 4 + j] for j in range(SLOTS)], axis=0
+        )
+        scale = lax.rsqrt(square * (1.0 / 2048.0) + NORM_EPS)
+        gate = jnp.minimum(dot(rows, wg[...]) * scale, GATE_LIMIT)
+        up = jnp.clip(dot(rows, wu[...]) * scale, -GATE_LIMIT, GATE_LIMIT)
+        act = ((up + 1.0) * gate * jax.nn.sigmoid(GATE_SLOPE * gate)).astype(BF16)
+        for j in range(N_TP):
+            terms = dot(act, wd[:, j * 512 : (j + 1) * 512]).astype(BF16)
+            for k in range(4):
+                down_send[n, j, k * 3 * NS : (k + 1) * 3 * NS, :] = terms[
+                    :, k * 128 : (k + 1) * 128
+                ]
+        for d in (2, 1, 3):
+            peer = lax.rem(tp + d, N_TP)
+            copy = pltpu.make_async_remote_copy(
+                src_ref=down_send.at[n, peer], dst_ref=down_recv.at[n, d - 1],
+                send_sem=d_ssem.at[n, d - 1], recv_sem=d_rsem.at[n, d - 1],
+                device_id={"tp": peer}, device_id_type=MESH,
+            )
+            copy.start()
+            d_copies.append(copy)
+
+    def back_copy(r):
+        return pltpu.make_async_remote_copy(
+            src_ref=send_b.at[r], dst_ref=recv_b.at[me],
+            send_sem=b_ssem, recv_sem=b_rsem,
+            device_id={"ep": lax.rem(me + r, N_EP)}, device_id_type=MESH,
+        )
+
+    for n, group in enumerate(ORDER):
+        for copy in d_copies[3 * n : 3 * n + 3]:
+            copy.wait_recv()
+        total = down_send[n, tp].astype(F32)
+        for d in range(N_TP - 1):
+            total = total + down_recv[n, d].astype(F32)
+        first = group * NS
+        send_b[first : first + NS] = (
+            dot(unpick[...], total.astype(BF16)).astype(BF16).reshape(NS, 16, 128)
+        )
+
+        def send_back(r, carry):
+            back_copy(r).start()
+            return carry
+
+        lax.fori_loop(max(1, first), first + NS, send_back, 0)
+    recv_b[me] = send_b[0]
+    some = pl.ds(0, N_EP - 1)
+    wait_bytes(recv_b.at[some], b_rsem)
+    result = dot(take[...], recv_b[...].reshape(N_EP * 16, 128))
+    for k in range(4):
+        part = result[k * 32 : (k + 1) * 32] + result[128 + k * 32 : 160 + k * 32]
+        out_ref[:, k * 128 : (k + 1) * 128] = (
+            residual[:, k * 128 : (k + 1) * 128] + part
+        ).astype(BF16)
+    for copy in g_copies + d_copies:
+        copy.wait_send()
+    wait_bytes(send_a.at[some], a_ssem)
+    wait_bytes(send_b.at[some], b_ssem)
+
+
+def tail(mixed, tokens, gain, routes, weight, wout, wg, wu, wd):
+    by_choice = routes.T
+    vmem = pl.BlockSpec(memory_space=pltpu.VMEM)
+    hbm = pl.BlockSpec(memory_space=pl.ANY)
+    dma = pltpu.SemaphoreType.DMA
+    return pl.pallas_call(
+        tail_kernel,
+        out_shape=jax.ShapeDtypeStruct((32, 512), BF16),
+        in_specs=[vmem] * 7 + [hbm] * 4,
+        out_specs=vmem,
+        scratch_shapes=[
+            pltpu.VMEM((256, 2048), BF16),
+            pltpu.VMEM((2048, 256), BF16),
+            pltpu.VMEM((2048, 256), BF16),
+            pltpu.VMEM((256, 2048), BF16),
+            pltpu.VMEM((1024, 256), BF16),
+            pltpu.VMEM((256, 1024), BF16),
+            pltpu.VMEM((PACKED, 16 * NS), BF16),
+            pltpu.VMEM((16 * NS, KEPT), BF16),
+            pltpu.VMEM((N_TP, 32, 512), BF16),
+            pltpu.VMEM((N_TP - 1, 32, 512), BF16),
+            pltpu.VMEM((32, 512), F32),
+            pltpu.VMEM((N_EP, 16, 128), BF16),
+            pltpu.VMEM((N_EP, 16, 128), BF16),
+            pltpu.VMEM((GROUPS, N_TP, PACKED, 128), BF16),
+            pltpu.VMEM((GROUPS, N_TP, KEPT, 128), BF16),
+            pltpu.VMEM((GROUPS, N_TP - 1, KEPT, 128), BF16),
+            pltpu.VMEM((N_EP, 16, 128), BF16),
+            pltpu.VMEM((N_EP, 16, 128), BF16),
+            dma((4,)),
+            dma((N_TP - 1,)),
+            dma((N_TP - 1,)),
+            dma,
+            dma((GROUPS,)),
+            dma((GROUPS, N_TP - 1)),
+            dma((GROUPS, N_TP - 1)),
+            dma((GROUPS, N_TP - 1)),
+            dma((GROUPS, N_TP - 1)),
+            dma,
+            dma,
+        ],
+        name="tail",
+        compiler_params=pltpu.CompilerParams(
+            collective_id=1, has_side_effects=True, vmem_limit_bytes=40 * 1024 * 1024
+        ),
+    )(
+        mixed, tokens, gain.reshape(N_TP, 512), routes, by_choice.reshape(1, 128),
+        jnp.tile(by_choice, (1, 8)), weight, wout, wg, wu, wd,
+    )
 
 def shards(
     tokens,
@@ -176,56 +447,10 @@
         head_norm_gain,
         state,
     )
-    head_terms = jnp.dot(mixed_inputs, output_weight, preferred_element_type=jnp.float32)
-    own_columns = tokens.shape[1]
-    column_start = lax.axis_index("tp") * own_columns
-    residual = present_rows.astype(jnp.float32) + of_everyone(
-        head_terms.astype(jnp.bfloat16), "tp"
-    ).astype(jnp.float32)
-    expert_rows = row_rescale(residual, second_norm_gain).astype(jnp.bfloat16)
-    residual_own = lax.dynamic_slice_in_dim(residual, column_start, own_columns, 1)
-    normed_own = lax.dynamic_slice_in_dim(expert_rows, column_start, own_columns, 1)
-    sequences, choices_per = routes.shape
-    experts = expert_gate_weight.shape[0] * lax.axis_size("ep")
-    capacity = max(2, 3 * sequences * choices_per // (2 * experts))
-    flattened = routes.reshape(-1)
-    onehot = (flattened[:, None] == jnp.arange(experts, dtype=jnp.int32)[None, :]).astype(jnp.int32)
-    ranking = jnp.sum((jnp.cumsum(onehot, axis=0) - onehot) * onehot, axis=1)
-    slot_index = flattened * capacity + ranking
-    placing = jnp.arange(experts * capacity, dtype=jnp.int32)[:, None] == slot_index[None, :]
-    dispatch = jnp.sum(
-        placing.reshape(experts * capacity, sequences, choices_per).astype(jnp.int32), axis=2
-    ).astype(jnp.bfloat16)
-    outgoing = jnp.dot(dispatch, normed_own, preferred_element_type=jnp.float32).astype(
-        jnp.bfloat16
-    )
-    outgoing = outgoing.reshape(experts, capacity, -1)
-    arrived = gather_directly(
-        lax.all_to_all(outgoing, "ep", split_axis=0, concat_axis=0, tiled=True), "tp", 2
-    )
-    sources, slot_count, feature_count = arrived.shape
-    expert_input = arrived.reshape(sources * slot_count, feature_count)
-    gate_pre = jnp.minimum(
-        jnp.dot(expert_input, expert_gate_weight[0], preferred_element_type=jnp.float32), GATE_LIMIT
-    )
-    up_pre = jnp.clip(
-        jnp.dot(expert_input, expert_up_weight[0], preferred_element_type=jnp.float32),
-        -GATE_LIMIT,
-        GATE_LIMIT,
-    )
-    activation = ((up_pre + 1.0) * gate_pre * jax.nn.sigmoid(GATE_SLOPE * gate_pre)).astype(
-        jnp.bfloat16
-    )
-    down_terms = jnp.dot(activation, expert_down_weight[0], preferred_element_type=jnp.float32)
-    down_terms = down_terms.reshape(sources, slot_count, -1)
-    shares = summed_on_arrival(down_terms.astype(jnp.bfloat16), "tp", 2).astype(jnp.bfloat16)
-    returned = lax.all_to_all(shares, "ep", split_axis=0, concat_axis=0, tiled=True)
-    returned_rows = returned.reshape(experts * capacity, -1)
-    picked = jnp.take(returned_rows, slot_index, axis=0).astype(jnp.float32)
-    weighted = jnp.sum(
-        picked.reshape(sequences, choices_per, -1) * chosen_expert_weight[:, :, None], axis=1
-    )
-    layer_out = (residual_own + weighted).astype(jnp.bfloat16)
+    layer_out = tail(
+        mixed_inputs, tokens, second_norm_gain, routes, chosen_expert_weight,
+        output_weight, expert_gate_weight, expert_up_weight, expert_down_weight,
+    )
     return (layer_out, new_state)
 
 

time: 126 us -> 94.7 us (0.75)
  blocking collectives: 68.4 us -> 11 us
  Pallas kernels: 0 us -> 51.1 us
  waiting for transfers between devices: 17.9 us -> 0 us
  starting transfers between devices: 9.55 us -> 0 us
  local copies, waits for them, and re-layouts: 9.45 us -> 13.6 us
  matrix products: 12.5 us -> 10.2 us
    all_to_all x3 -> x0, blocking collectives: 57.4 us -> none  [the longest x1 29.1 us: shards(): lax.all_to_all(outgoing, 'ep', split_axis=0, concat_axis=0, tiled=True)]
    pallas_call x0 -> x1, Pallas kernels: none -> 51.1 us  [tail(): pl.pallas_call(tail_kernel, out_shape=jax.ShapeDtypeStruct((32, 512), BF1...]
    all_to_all x2 -> x0, waiting for transfers between devices: 17.9 us -> none  [the longest x1 12.7 us: shards(): lax.all_to_all(shares, 'ep', split_axis=0, concat_axis=0, tiled=True)]
    all_to_all x2 -> x0, starting transfers between devices: 9.55 us -> none  [the longest x1 6.08 us: shards(): lax.all_to_all(shares, 'ep', split_axis=0, concat_axis=0, tiled=True)]
    unnamed x35 -> x25, local copies, waits for them, and re-layouts: 2.4 us -> 6.63 us
    add x1, other arithmetic: 2.81 us -> 4.56 us  [head_combiner(): state * decay[:, :, None, :]]
    dot_general x5 -> x0, matrix products: 1.69 us -> none  [the longest x1 0.38 us: shards(): jnp.dot(expert_input, expert_up_weight[0], preferred_element_type=jnp.flo...]
  transfers between devices with their start and end apart: 2 -> 0, of which waited for: 2 -> 0; matrix products, arithmetic and copies ran while one was open for 2% -> 0% of each run, Pallas kernels for 0% -> 0%
where the time goes in v1:
time: 94.7 us; the launch traced here: 93.9 us
  Pallas kernels  51.1 us (54%)
  local copies, waits for them, and re-layouts  13.6 us (14%)
  blocking collectives  11 us (12%)
  matrix products  10.2 us (11%)
  other arithmetic  7.24 us (8%)
    pallas_call x1, Pallas kernels, tail(): pl.pallas_call(tail_kernel, out_shape=jax.ShapeDtypeStruct((32, 512), BF1...  51.1 us
    all_gather x1, blocking collectives, in_one_piece(): result = lax.all_gather(both, axis, axis=dim, tiled=True)  11 us
    unnamed x25, local copies, waits for them, and re-layouts  6.63 us
    dot_general x5, matrix products, project(): return jnp.dot(inputs, weight, preferred_element_type=jnp.float32)  5.64 us
    add x1, other arithmetic, head_combiner(): state * decay[:, :, None, :]  4.56 us
    dot_general x1, matrix products, head_combiner(): along = jnp.einsum('shij,shj->shi', state, removal)  3.36 us

profile of v1, /device:TPU:1, one launch (start us, length us, event | category | flops | bytes accessed | tf_op | source)
XLA Modules:
  0.0 93.9 jit_solution(5213764895431633703)
XLA Ops:
  0.7 0.9 reshape.89.routes_row_ref
  1.6 0.8 mul.222
  2.4 0.8 mul.240
  3.1 1.3 %mul.252 = f32[4,64]{1,0:T(4,128)} reshape(f32[256]{0:T(256)} %param.39) | data formatting | bytes 2048 | tf_op jit(solution)/shard_map/mul | solution.py:81
  4.5 0.7 reshape.88.gain_ref
  5.2 0.8 copy.27.weight_ref
  5.9 0.7 tile.4
  6.7 0.8 copy.26.routes_ref
  7.5 1.1 %fusion.82 = (f32[1,2048]{1,0:T(1,128)S(1)}, f32[1,2048]{1,0:T(1,128)S(1)}, f32[1,2048]{1,0:T(1,128)S(1)}, f32[1,2048]{1,0:T(1,128)S(1)}, f32[1,2048]{1,0:T(1,128)S(1)}) fusion(f32[5,2048]{1,0:T(8,128)} %param.27), kind=kLoop, calls=%fused_computation.79 | loop fusion | bytes 81920 | tf_op jit(solution)/shard_map/slice | solution.py:52
  8.5 0.8 pad_maximum_fusion
  9.3 11.0 %all_gather.3 = bf16[64,2048]{1,0:T(8,128)(2,1)S(1)} all-gather(bf16[64,512]{1,0:T(8,128)(2,1)S(1)} %pad_maximum_fusion), channel_id=1, replica_groups=mesh['ep'=64,'tp'=4] {'tp'}, dimensions={1}, use_global_device_ids=true | all-gather | bytes 327680 | tf_op jit(solution)/shard_map/all_gather | solution.py:18
  20.4 1.0 %fusion.22 = f32[32,256]{1,0:T(8,128)S(1)} fusion(bf16[2048,256]{1,0:T(8,128)(2,1)S(1)} %copy-done, f32[2048]{0:T(1024)S(1)} %bitcast.31, f32[2048]{0:T(1024)} %param.26, f32[32]{0:T(128)S(1)} %add_rsqrt_fusion.2, bf16[64,2048]{1,0:T(8,128)(2,1)S(1)} %all_gather.3), kind=kOutput, calls=%fused_computation.29 | convolution fusion | flops 34078720 | bytes 1360000 | tf_op jit(solution)/shard_map/dot_general | solution.py:55
  21.4 1.6 %fusion.24 = f32[32,256]{1,0:T(8,128)S(1)} fusion(bf16[2048,256]{1,0:T(8,128)(2,1)} %param.30, f32[2048]{0:T(1024)S(1)} %bitcast.30, f32[2048]{0:T(1024)} %param.26, f32[32]{0:T(128)S(1)} %add_rsqrt_fusion.2, bf16[64,2048]{1,0:T(8,128)(2,1)S(1)} %all_gather.3), kind=kOutput, calls=%fused_computation.30 | convolution fusion | flops 34078720 | bytes 1360000 | tf_op jit(solution)/shard_map/dot_general | solution.py:55
  23.0 1.4 %fusion.6 = f32[32,256]{1,0:T(8,128)S(1)} fusion(bf16[2048,128]{1,0:T(8,128)(2,1)} %param.34, f32[2048]{0:T(1024)S(1)} %bitcast.35, f32[2048]{0:T(1024)} %param.26, f32[32]{0:T(128)S(1)} %add_rsqrt_fusion.2, bf16[64,2048]{1,0:T(8,128)(2,1)S(1)} %all_gather.3, bf16[128,1024]{1,0:T(8,128)(2,1)} %param.35, s32[]{:T(128)S(6)} %select_n.8), kind=kOutput, calls=%fused_computation.8 | convolution fusion | flops 19427328 | bytes 901252 | tf_op jit(solution)/shard_map/dot_general | solution.py:55
  24.5 1.3 %fusion.73 = f32[32,256]{1,0:T(8,128)S(1)} fusion(bf16[128,1024]{1,0:T(8,128)(2,1)} %param.32, s32[]{:T(128)S(6)} %select_n.8, bf16[2048,128]{1,0:T(8,128)(2,1)S(1)} %copy-done.9, f32[2048]{0:T(1024)S(1)} %bitcast.34, f32[2048]{0:T(1024)S(1)} %copy-done.8, f32[32]{0:T(128)S(1)} %add_rsqrt_fusion.2, bf16[64,2048]{1,0:T(8,128)(2,1)S(1)} %all_gather.3, ...), kind=kOutput, calls=%fused_computation.70 | convolution fusion | flops 19492864 | bytes 902276 | tf_op jit(solution)/shard_map/dot_general | solution.py:55
  26.7 3.4 %fusion.83 = f32[32,4,1,64]{3,2,1,0:T(1,128)S(1)} fusion(f32[32,4,64,1]{2,3,1,0:T(1,128)S(1)} %bitcast.28, f32[32,4,64,64]{3,2,1,0:T(8,128)} %param.41), kind=kOutput, calls=%fused_computation.80 | convolution fusion | flops 1048576 | bytes 2162688 | tf_op jit(solution)/shard_map/shij,shj->shi/dot_general | solution.py:71
  30.3 4.6 %multiply_add_fusion = f32[32,4,64,64]{3,2,1,0:T(8,128)S(1)} fusion(f32[32,4,64,64]{3,2,1,0:T(8,128)} %param.41, f32[32,4,64]{2,1,0:T(4,128)S(1)} %get-tuple-element.4, f32[32,4,64]{2,1,0:T(4,128)S(1)} %mul.238, f32[32,4,64]{2,1,0:T(4,128)S(1)} %get-tuple-element.2, f32[32,4,64]{2,1,0:T(4,128)S(1)} %bitcast.26, f32[32,4,64]{2,1,0:T(4,128)S(1)} %mul.216), kind=kLoop, calls=%fused_computation.1 | loop fusion | flops 2621440 | bytes 4358144 | tf_op jit(solution)/shard_map/add | solution.py:73
  34.9 2.0 %copy-done.6 = f32[32,4,64,64]{3,2,1,0:T(8,128)} copy-done((f32[32,4,64,64]{3,2,1,0:T(8,128)}, f32[32,4,64,64]{3,2,1,0:T(8,128)S(1)}, u32[]{:S(2)}) %copy-start.6) | copy-done | bytes 2097176
  36.9 1.2 %fusion.84 = f32[32,4,1,64]{3,2,1,0:T(1,128)S(1)} fusion(f32[32,4,64,64]{3,2,1,0:T(8,128)S(1)} %multiply_add_fusion, f32[32,4,64,1]{2,3,1,0:T(1,128)S(1)} %bitcast.27), kind=kOutput, calls=%fused_computation.81 | convolution fusion | flops 1048576 | bytes 2162688 | tf_op jit(solution)/shard_map/shij,shj->shi/dot_general | solution.py:77
  38.4 1.2 %fusion.3 = bf16[32,4,64]{2,1,0:T(4,128)(2,1)S(1)} fusion(f32[32,4,64]{2,1,0:T(4,128)S(1)} %mul.238, f32[32,4,64]{2,1,0:T(4,128)S(1)} %bitcast.25, f32[4,64]{1,0:T(4,128)} %mul.252, f32[32,4]{1,0:T(8,128)S(1)} %add_rsqrt_fusion, f32[32,4]{1,0:T(8,128)S(1)} %broadcast_multiply_fusion, f32[32,4,64]{2,1,0:T(4,128)S(1)} %reshape.87, ...), kind=kOutput, calls=%fused_computation.4 | output fusion | flops 65727 | bytes 150528 | tf_op jit(solution)/shard_map/mul | solution.py:86
  39.8 1.2 %copy-done.3 = bf16[1,2048,256]{2,1,0:T(8,128)(2,1)S(1)} copy-done((bf16[1,2048,256]{2,1,0:T(8,128)(2,1)S(1)}, bf16[1,2048,256]{2,1,0:T(8,128)(2,1)}, u32[]{:S(2)}) %copy-start.3) | copy-done | bytes 1048600
  41.0 1.2 %copy-done.4 = bf16[1,256,2048]{2,1,0:T(8,128)(2,1)S(1)} copy-done((bf16[1,256,2048]{2,1,0:T(8,128)(2,1)S(1)}, bf16[1,256,2048]{2,1,0:T(8,128)(2,1)}, u32[]{:S(2)}) %copy-start.4) | copy-done | bytes 1048600
  42.2 51.1 %tail.1 = bf16[32,512]{1,0:T(8,128)(2,1)S(1)} custom-call(bf16[32,256]{1,0:T(8,128)(2,1)S(1)} %convert_element_type.42.mixed_ref, bf16[32,512]{1,0:T(8,128)(2,1)S(1)} %copy-done.5, f32[4,512]{1,0:T(4,128)S(1)} %reshape.88.gain_ref, s32[32,4]{1,0:T(8,128)S(1)} %copy.26.routes_ref, s32[1,128]{1,0:T(1,128)S(1)} %reshape.89.routes_row_ref, ...), custom_call_target="tpu_custom_call" | custom-call | tf_op jit(solution)/shard_map/tail/pallas_call | solution.py:355
  93.3 0.6 copy.33
  (37 shorter events, 1.8 us)
Async XLA Ops:
  0.6 19.8 %copy-start = (bf16[2048,256]{1,0:T(8,128)(2,1)S(1)}, bf16[2048,256]{1,0:T(8,128)(2,1)}, u32[]{:S(2)}) copy-start(bf16[2048,256]{1,0:T(8,128)(2,1)} %param.28) | copy-start | bytes 3145732
  0.6 23.8 %copy-start.8 = (f32[2048]{0:T(1024)S(1)}, f32[2048]{0:T(1024)}, u32[]{:S(2)}) copy-start(f32[2048]{0:T(1024)} %param.26) | copy-start | bytes 24580
  0.7 23.8 %copy-start.10 = (f32[256]{0:T(256)S(1)}, f32[256]{0:T(256)}, u32[]{:S(2)}) copy-start(f32[256]{0:T(256)} %param.33) | copy-start | bytes 3076
  0.7 23.8 %copy-start.9 = (bf16[2048,128]{1,0:T(8,128)(2,1)S(1)}, bf16[2048,128]{1,0:T(8,128)(2,1)}, u32[]{:S(2)}) copy-start(bf16[2048,128]{1,0:T(8,128)(2,1)} %param.31) | copy-start | bytes 1572868
  0.7 25.1 %copy-start.7 = (bf16[2048,256]{1,0:T(8,128)(2,1)S(1)}, bf16[2048,256]{1,0:T(8,128)(2,1)}, u32[]{:S(2)}) copy-start(bf16[2048,256]{1,0:T(8,128)(2,1)} %param.29) | copy-start | bytes 3145732
  34.9 2.0 %copy-start.6 = (f32[32,4,64,64]{3,2,1,0:T(8,128)}, f32[32,4,64,64]{3,2,1,0:T(8,128)S(1)}, u32[]{:S(2)}) copy-start(f32[32,4,64,64]{3,2,1,0:T(8,128)S(1)} %multiply_add_fusion) | copy-start | bytes 6291460
  36.9 2.9 %copy-start.1 = (bf16[256,2048]{1,0:T(8,128)(2,1)S(1)}, bf16[256,2048]{1,0:T(8,128)(2,1)}, u32[]{:S(2)}) copy-start(bf16[256,2048]{1,0:T(8,128)(2,1)} %wout_hbm.1) | copy-start | bytes 3145732
  36.9 2.9 %copy-start.2 = (bf16[1,2048,256]{2,1,0:T(8,128)(2,1)S(1)}, bf16[1,2048,256]{2,1,0:T(8,128)(2,1)}, u32[]{:S(2)}) copy-start(bf16[1,2048,256]{2,1,0:T(8,128)(2,1)} %wg_hbm.1) | copy-start | bytes 3145732
  36.9 2.9 %copy-start.5 = (bf16[32,512]{1,0:T(8,128)(2,1)S(1)}, bf16[32,512]{1,0:T(8,128)(2,1)}, u32[]{:S(2)}) copy-start(bf16[32,512]{1,0:T(8,128)(2,1)} %tokens_ref.1) | copy-start | bytes 98308
  39.8 1.2 %copy-start.3 = (bf16[1,2048,256]{2,1,0:T(8,128)(2,1)S(1)}, bf16[1,2048,256]{2,1,0:T(8,128)(2,1)}, u32[]{:S(2)}) copy-start(bf16[1,2048,256]{2,1,0:T(8,128)(2,1)} %wu_hbm.1) | copy-start | bytes 3145732
  41.0 1.2 %copy-start.4 = (bf16[1,256,2048]{2,1,0:T(8,128)(2,1)S(1)}, bf16[1,256,2048]{2,1,0:T(8,128)(2,1)}, u32[]{:S(2)}) copy-start(bf16[1,256,2048]{2,1,0:T(8,128)(2,1)} %wd_hbm.1) | copy-start | bytes 3145732

commit v2 on v1

--- a/solution.py
+++ b/solution.py
@@ -10,88 +10,6 @@
 KEY_EPS = 1e-06
 GATE_LIMIT = 7.0
 GATE_SLOPE = 1.702
-
-
-def in_one_piece(arrays, axis, dim, along):
-    widths = [a.shape[along] for a in arrays]
-    both = jnp.concatenate(arrays, axis=along)
-    result = lax.all_gather(both, axis, axis=dim, tiled=True)
-    return tuple(jnp.split(result, [sum(widths[:k]) for k in range(1, len(widths))], axis=along))
-
-
-def row_rescale(values, gain):
-    return values * lax.rsqrt(jnp.mean(values * values, axis=-1, keepdims=True) + NORM_EPS) * gain
-
-
-def head_combiner(
-    present_rows,
-    prior_rows,
-    first_norm_gain,
-    token_shift_share,
-    receptance_weight,
-    key_weight,
-    value_weight,
-    decay_down_map,
-    decay_up_map,
-    decay_offset,
-    strength_down_map,
-    strength_up_map,
-    removal_key_scale,
-    key_damping,
-    self_term_weight,
-    head_norm_gain,
-    state,
-):
-    sequence_count = present_rows.shape[0]
-    head_number = state.shape[1]
-    head_extent = state.shape[2]
-    normed = row_rescale(present_rows.astype(jnp.float32), first_norm_gain)
-    before = prior_rows.astype(jnp.float32)
-
-    def shifted(role):
-        return (normed + (before - normed) * token_shift_share[role]).astype(jnp.bfloat16)
-
-    def project(inputs, weight):
-        return jnp.dot(inputs, weight, preferred_element_type=jnp.float32)
-
-    def by_heads(values):
-        return values.reshape(sequence_count, head_number, head_extent)
-
-    receptance_rows = by_heads(project(shifted(0), receptance_weight))
-    key_rows = by_heads(project(shifted(1), key_weight))
-    value_matrix = by_heads(project(shifted(2), value_weight))
-    decay_low = jnp.tanh(project(shifted(3), decay_down_map)).astype(jnp.bfloat16)
-    decay_pre = decay_offset + project(decay_low, decay_up_map)
-    decay = by_heads(jnp.exp(-jnp.exp(-jax.nn.softplus(-decay_pre) - 0.5)))
-    alpha_low = project(shifted(4), strength_down_map).astype(jnp.bfloat16)
-    alpha = by_heads(jax.nn.sigmoid(project(alpha_low, strength_up_map)))
-    removal = key_rows * removal_key_scale.reshape(head_number, head_extent)
-    removal = removal * lax.rsqrt(jnp.sum(removal * removal, axis=-1, keepdims=True) + KEY_EPS)
-    blended_rows = key_rows * (1.0 + (alpha - 1.0) * key_damping.reshape(head_number, head_extent))
-    along = jnp.einsum("shij,shj->shi", state, removal)
-    new_state = (
-        state * decay[:, :, None, :]
-        - along[..., None] * (removal * alpha)[:, :, None, :]
-        + value_matrix[..., None] * blended_rows[:, :, None, :]
-    )
-    readout = jnp.einsum("shij,shj->shi", new_state, receptance_rows)
-    centered = readout - jnp.mean(readout, axis=-1, keepdims=True)
-    variance = jnp.mean(centered * centered, axis=-1, keepdims=True)
-    heads_normalised = (
-        centered
-        * lax.rsqrt(variance + GROUP_EPS)
-        * head_norm_gain.reshape(head_number, head_extent)
-    )
-    self_term = (
-        jnp.sum(receptance_rows * blended_rows * self_term_weight, axis=-1, keepdims=True)
-        * value_matrix
-    )
-    mixed_inputs = (
-        (heads_normalised + self_term)
-        .reshape(sequence_count, head_number * head_extent)
-        .astype(jnp.bfloat16)
-    )
-    return (mixed_inputs, new_state)
 
 
 MESH = pl.DeviceIdType.MESH
@@ -107,6 +25,10 @@
 BF16 = jnp.bfloat16
 
 
+def pin(value):
+    return pltpu.with_memory_space_constraint(value, pltpu.HBM)
+
+
 def dot(a, b):
     return jnp.dot(a, b, preferred_element_type=F32)
 
@@ -123,16 +45,105 @@
     return jnp.where(m == 12, 3, m + third(m))
 
 
-def tail_kernel(
-    mixed_ref, tokens_ref, gain_ref, routes_ref, routes_row_ref, routes_tiled_ref, weight_ref,
+def gather_kernel(tokens_hbm, previous_hbm, rows_ref, load_sem, send_sem, recv_sem):
+    tp = lax.axis_index("tp")
+    loads = [
+        pltpu.make_async_copy(tokens_hbm, rows_ref.at[tp, pl.ds(0, 32)], load_sem.at[0]),
+        pltpu.make_async_copy(previous_hbm, rows_ref.at[tp, pl.ds(32, 32)], load_sem.at[1]),
+    ]
+    for load in loads:
+        load.start()
+    barrier = pltpu.get_barrier_semaphore()
+    for d in range(1, N_TP):
+        pl.semaphore_signal(
+            barrier, inc=1, device_id={"tp": lax.rem(tp + d, N_TP)}, device_id_type=MESH
+        )
+    for load in loads:
+        load.wait()
+    pl.semaphore_wait(barrier, N_TP - 1)
+    copies = []
+    for d in (2, 1, 3):
+        copy = pltpu.make_async_remote_copy(
+            src_ref=rows_ref.at[tp], dst_ref=rows_ref.at[tp],
+            send_sem=send_sem.at[d - 1], recv_sem=recv_sem.at[d - 1],
+            device_id={"tp": lax.rem(tp + d, N_TP)}, device_id_type=MESH,
+        )
+        copy.start()
+        copies.append(copy)
+    for copy in copies:
+        copy.wait()
+
+
+def gather(tokens, previous):
+    hbm = pl.BlockSpec(memory_space=pltpu.HBM)
+    dma = pltpu.SemaphoreType.DMA
+    return pl.pallas_call(
+        gather_kernel,
+        out_shape=jax.ShapeDtypeStruct((N_TP, 64, 512), BF16),
+        in_specs=[hbm, hbm],
+        out_specs=pl.BlockSpec(memory_space=pltpu.VMEM),
+        scratch_shapes=[dma((2,)), dma((N_TP - 1,)), dma((N_TP - 1,))],
+        name="gather",
+        compiler_params=pltpu.CompilerParams(
+            collective_id=0, has_side_effects=True, vmem_limit_bytes=4 * 1024 * 1024
+        ),
+    )(tokens, previous)
+
+
+def head_sums(values):
+    same = iota((256, 256), 0) // 64 == iota((256, 256), 1) // 64
+    return jnp.dot(
+        values, same.astype(F32), preferred_element_type=F32, precision=lax.Precision.HIGHEST
+    )
+
+
+def column(row):
+    eye = iota((32, 32), 0) == iota((32, 32), 1)
+    return jnp.sum(jnp.where(eye, row, jnp.zeros_like(row)), axis=1, keepdims=True)
+
+
+def layer_kernel(
+    rows_ref,
+    gain_one_hbm, share_hbm, offset_hbm, key_scale_hbm, damping_hbm, self_hbm, head_gain_hbm,
+    gain_hbm, routes_hbm, weight_hbm,
+    wr_hbm, wk_hbm, wv_hbm, dd_hbm, du_hbm, sd_hbm, su_hbm, state_hbm,
     wout_hbm, wg_hbm, wu_hbm, wd_hbm,
-    out_ref,
+    out_ref, state,
+    gain_one_ref, share_ref, offset_ref, key_scale_ref, damping_ref, self_pair, head_gain_ref,
+    gain_ref, routes_ref, weight_ref, self_ref, routes_row_ref, routes_tiled_ref,
+    wr, wk, wv, dd, du, sd, su, along_scr, query_scr, rows_scr,
     wout, wg, wu, wd, place, take, pick, unpick,
     rs_send, rs_recv, residual, send_a, recv_a, gathered, down_send, down_recv, send_b, recv_b,
-    w_sem, rs_ssem, rs_rsem, a_ssem, a_rsem, g_ssem, g_rsem, d_ssem, d_rsem, b_ssem, b_rsem,
+    w_sem, h_sem, p_sem, rs_ssem, rs_rsem, a_ssem, a_rsem, g_ssem, g_rsem, d_ssem, d_rsem, b_ssem, b_rsem,
 ):
     me = lax.axis_index("ep")
     tp = lax.axis_index("tp")
+    own = pl.ds(pl.multiple_of(tp * 256, 256), 256)
+    small_loads = [
+        pltpu.make_async_copy(source, target, p_sem.at[n])
+        for n, (source, target) in enumerate(
+            [
+                (gain_one_hbm, gain_one_ref), (share_hbm, share_ref), (offset_hbm, offset_ref),
+                (key_scale_hbm, key_scale_ref), (damping_hbm, damping_ref), (self_hbm, self_pair),
+                (head_gain_hbm, head_gain_ref),
+                (gain_hbm.at[:, pl.ds(pl.multiple_of(tp * 512, 512), 512)], gain_ref),
+                (routes_hbm, routes_ref), (weight_hbm, weight_ref),
+            ]
+        )
+    ]
+    for load in small_loads:
+        load.start()
+    head_loads = [
+        pltpu.make_async_copy(source, target, h_sem.at[n])
+        for n, (source, target) in enumerate(
+            [
+                (dd_hbm, dd), (sd_hbm, sd), (wk_hbm, wk), (wr_hbm, wr), (wv_hbm, wv),
+                (du_hbm.at[:, own], du), (su_hbm.at[:, own], su), (state_hbm, state),
+            ]
+        )
+    ]
+    for load in head_loads:
+        load.start()
     loads = [
         pltpu.make_async_copy(wout_hbm, wout, w_sem.at[0]),
         pltpu.make_async_copy(wg_hbm.at[0], wg, w_sem.at[1]),
@@ -155,9 +166,73 @@
 
     lax.fori_loop(1, N_EP, greet, 0)
 
+    for load in small_loads:
+        load.wait()
+    for h in range(4):
+        self_ref[:, h * 64 : (h + 1) * 64] = self_pair[h : h + 1, :]
+    for c in range(4):
+        routes_row_ref[:, c * 32 : (c + 1) * 32] = routes_ref[c : c + 1, :]
+    for b in range(8):
+        routes_tiled_ref[:, b * 32 : (b + 1) * 32] = routes_ref[...]
+    square = jnp.zeros((32, 1), F32)
+    for t in range(N_TP):
+        part = rows_ref[t, 0:32, :].astype(F32)
+        square = square + jnp.sum(part * part, axis=1, keepdims=True)
+    scale = lax.rsqrt(square * (1.0 / 2048.0) + NORM_EPS)
+    sums = [None] * 5
+    for t in range(N_TP):
+        span = slice(t * 512, (t + 1) * 512)
+        normed = rows_ref[t, 0:32, :].astype(F32) * scale * gain_one_ref[:, span]
+        change = rows_ref[t, 32:64, :].astype(F32) - normed
+        for n, (m, weight) in enumerate([(3, dd), (4, sd), (1, wk), (0, wr), (2, wv)]):
+            if t == 0:
+                head_loads[n].wait()
+            shifted = (normed + change * share_ref[m : m + 1, span]).astype(BF16)
+            term = dot(shifted, weight[span, :])
+            sums[n] = term if t == 0 else sums[n] + term
+    low, strength_low, key, receptance, value = sums
+    head_loads[5].wait()
+    decay = dot(jnp.tanh(low).astype(BF16), du[...]) + offset_ref[...]
+    decay = jnp.exp(jax.nn.sigmoid(decay) * -(2.718281828459045 ** -0.5))
+    head_loads[6].wait()
+    alpha = jax.nn.sigmoid(dot(strength_low.astype(BF16), su[...]))
+    removal = key * key_scale_ref[...]
+    removal = removal * lax.rsqrt(head_sums(removal * removal) + KEY_EPS)
+    blended = key * (1.0 + (alpha - 1.0) * damping_ref[...])
+    strong = removal * alpha
+    query = decay * receptance
+    both = head_sums(
+        jnp.concatenate(
+            [strong * receptance, blended * receptance, blended * receptance * self_ref[...]], axis=0
+        )
+    )
+    head_loads[7].wait()
+    for h in range(4):
+        lanes = slice(h * 64, (h + 1) * 64)
+        asked = jnp.concatenate([removal[:, lanes], query[:, lanes]], axis=0).astype(BF16)
+        for q in range(8):
+            held = state[4 * q : 4 * q + 4, h].reshape(256, 64).astype(BF16)
+            answer = lax.dot_general(
+                asked, held, (((1,), (1,)), ((), ())), preferred_element_type=F32
+            )
+            for j in range(4):
+                s = 4 * q + j
+                span = slice(j * 64, (j + 1) * 64)
+                along_scr[s : s + 1, lanes] = answer[s : s + 1, span]
+                query_scr[s : s + 1, lanes] = answer[32 + s : 33 + s, span]
+    along = along_scr[...]
+    readout = query_scr[...] - along * both[0:32] + value * both[32:64]
+    centred = readout - head_sums(readout) * (1.0 / 64.0)
+    spread = head_sums(centred * centred) * (1.0 / 64.0)
+    mixed = centred * lax.rsqrt(spread + GROUP_EPS) * head_gain_ref[...] + both[64:96] * value
+    mixed = mixed.astype(BF16)
+    for n, values in enumerate((-along, value, strong, blended, decay)):
+        for h in range(4):
+            rows_scr[n, h] = values[:, h * 64 : (h + 1) * 64]
+
     loads[0].wait()
     for j in range(N_TP):
-        rs_send[j] = dot(mixed_ref[...], wout[:, j * 512 : (j + 1) * 512]).astype(BF16)
+        rs_send[j] = dot(mixed, wout[:, j * 512 : (j + 1) * 512]).astype(BF16)
     pl.semaphore_wait(barrier, N_EP - 1 + N_TP - 1)
     rs_copies = []
     for d in (2, 1, 3):
@@ -173,12 +248,13 @@
     lane = iota((1, 256), 1)
     block, seq = lane // 32, lane % 32
     source = iota((32, 256), 0)
+    routed = [column(routes_ref[c : c + 1, :]) for c in range(4)]
     targets = []
     for c in range(4):
         mine = routes_tiled_ref[c : c + 1, :]
         rank = jnp.zeros((1, 256), jnp.int32)
         for other in range(c + 1):
-            same = routes_ref[:, other : other + 1] == mine
+            same = routed[other] == mine
             if other == c:
                 same = same & (source < seq)
             rank = rank + jnp.sum(same.astype(jnp.int32), axis=0, keepdims=True)
@@ -203,14 +279,14 @@
 
     for copy in rs_copies:
         copy.wait()
-    total = tokens_ref[...].astype(F32) + rs_send[tp].astype(F32)
+    total = rows_ref[tp, 0:32, :].astype(F32) + rs_send[tp].astype(F32)
     for d in range(N_TP - 1):
         total = total + rs_recv[d].astype(F32)
     residual[...] = total
     square = jnp.sum(total * total, axis=1, keepdims=True)
     high = square.astype(BF16).astype(F32)
     low = square - high
-    scaled = total * gain_ref[pl.ds(tp, 1), :]
+    scaled = total * gain_ref[...]
     stack = [scaled[:, k * 128 : (k + 1) * 128] for k in range(4)]
     sum_lane = iota((32, 128), 1)
     for j in range(SLOTS):
@@ -240,20 +316,40 @@
     earlier = iota((32, 128), 1)
     columns = []
     for c in range(4):
-        mine = routes_ref[:, c : c + 1]
+        mine = routed[c]
         same = (routes_row_ref[...] == mine) & (earlier < c * 32 + seq_col)
         columns.append(mine * 16 + jnp.sum(same.astype(jnp.int32), axis=1, keepdims=True))
+    weights = [column(weight_ref[c : c + 1, :]) for c in range(4)]
     for k in range(4):
         for j in range(8):
             at = iota((32, 128), 1) + (j * 128 - k * 4)
             share = jnp.zeros((32, 128), F32)
             for c in range(4):
-                share = jnp.where(at == columns[c], weight_ref[:, c : c + 1], share)
+                share = jnp.where(at == columns[c], weights[c], share)
             upper = share.astype(BF16)
             take[k * 32 : (k + 1) * 32, j * 128 : (j + 1) * 128] = upper
             take[128 + k * 32 : 160 + k * 32, j * 128 : (j + 1) * 128] = (
                 share - upper.astype(F32)
             ).astype(BF16)
+
+    upper_row = iota((8, 64), 0)
+
+    def renew(s, carry):
+        for h in range(4):
+            minus, given, strong_row, blended_row, decay_row = [
+                rows_scr[n, h, pl.ds(s, 1), :] for n in range(5)
+            ]
+            zero = jnp.zeros((8, 64), F32)
+            left = jnp.where(upper_row == 0, minus, jnp.where(upper_row == 1, given, zero))
+            right = jnp.where(upper_row == 0, strong_row, jnp.where(upper_row == 1, blended_row, zero))
+            change = lax.dot_general(
+                left, right, (((0,), (0,)), ((), ())),
+                preferred_element_type=F32, precision=lax.Precision.HIGHEST,
+            )
+            state[s, h] = state[s, h] * decay_row + change
+        return carry
+
+    lax.fori_loop(0, 32, renew, 0)
 
     def wait_bytes(ref, sem):
         pltpu.make_async_copy(ref, ref, sem).wait()
@@ -347,17 +443,45 @@
     wait_bytes(send_b.at[some], b_ssem)
 
 
-def tail(mixed, tokens, gain, routes, weight, wout, wg, wu, wd):
-    by_choice = routes.T
+def layer(
+    rows, gain_one, share, offset, key_scale, damping, self_weight, head_gain, gain, routes, weight,
+    wr, wk, wv, dd, du, sd, su, state, wout, wg, wu, wd,
+):
     vmem = pl.BlockSpec(memory_space=pltpu.VMEM)
-    hbm = pl.BlockSpec(memory_space=pl.ANY)
+    hbm = pl.BlockSpec(memory_space=pltpu.HBM)
     dma = pltpu.SemaphoreType.DMA
     return pl.pallas_call(
-        tail_kernel,
-        out_shape=jax.ShapeDtypeStruct((32, 512), BF16),
-        in_specs=[vmem] * 7 + [hbm] * 4,
-        out_specs=vmem,
+        layer_kernel,
+        out_shape=(
+            pltpu.VMEM((32, 512), BF16),
+            pltpu.VMEM((32, 4, 64, 64), F32),
+        ),
+        in_specs=[vmem] + [hbm] * 22,
+        out_specs=(vmem, vmem),
         scratch_shapes=[
+            pltpu.VMEM((1, 2048), F32),
+            pltpu.VMEM((5, 2048), F32),
+            pltpu.VMEM((1, 256), F32),
+            pltpu.VMEM((1, 256), F32),
+            pltpu.VMEM((1, 256), F32),
+            pltpu.VMEM((4, 64), F32),
+            pltpu.VMEM((1, 256), F32),
+            pltpu.VMEM((1, 512), F32),
+            pltpu.VMEM((4, 32), jnp.int32),
+            pltpu.VMEM((4, 32), F32),
+            pltpu.VMEM((1, 256), F32),
+            pltpu.VMEM((1, 128), jnp.int32),
+            pltpu.VMEM((4, 256), jnp.int32),
+            pltpu.VMEM((2048, 256), BF16),
+            pltpu.VMEM((2048, 256), BF16),
+            pltpu.VMEM((2048, 256), BF16),
+            pltpu.VMEM((2048, 128), BF16),
+            pltpu.VMEM((128, 256), BF16),
+            pltpu.VMEM((2048, 128), BF16),
+            pltpu.VMEM((128, 256), BF16),
+            pltpu.VMEM((32, 256), F32),
+            pltpu.VMEM((32, 256), F32),
+            pltpu.VMEM((5, 4, 32, 64), F32),
             pltpu.VMEM((256, 2048), BF16),
             pltpu.VMEM((2048, 256), BF16),
             pltpu.VMEM((2048, 256), BF16),
@@ -377,6 +501,8 @@
             pltpu.VMEM((N_EP, 16, 128), BF16),
             pltpu.VMEM((N_EP, 16, 128), BF16),
             dma((4,)),
+            dma((8,)),
+            dma((10,)),
             dma((N_TP - 1,)),
             dma((N_TP - 1,)),
             dma,
@@ -388,14 +514,16 @@
             dma,
             dma,
         ],
-        name="tail",
+        name="layer",
         compiler_params=pltpu.CompilerParams(
-            collective_id=1, has_side_effects=True, vmem_limit_bytes=40 * 1024 * 1024
+            collective_id=1, has_side_effects=True, vmem_limit_bytes=48 * 1024 * 1024
         ),
     )(
-        mixed, tokens, gain.reshape(N_TP, 512), routes, by_choice.reshape(1, 128),
-        jnp.tile(by_choice, (1, 8)), weight, wout, wg, wu, wd,
+        rows, *map(pin, (gain_one.reshape(1, 2048), share, offset.reshape(1, 256), key_scale.reshape(1, 256),
+        damping.reshape(1, 256), self_weight, head_gain.reshape(1, 256),
+        gain.reshape(1, 2048), routes.T, weight.T, wr, wk, wv, dd, du, sd, su, state, wout, wg, wu, wd))
     )
+
 
 def shards(
     tokens,
@@ -423,35 +551,13 @@
     expert_up_weight,
     expert_down_weight,
 ):
-    present_rows, prior_rows = in_one_piece((tokens, previous), "tp", 1, 0)
-    head_columns = receptance_weight.shape[1]
-    head_start = lax.axis_index("tp") * head_columns
-    decay_own = lax.dynamic_slice_in_dim(decay_up_map, head_start, head_columns, 1)
-    alpha_own = lax.dynamic_slice_in_dim(strength_up_map, head_start, head_columns, 1)
-    mixed_inputs, new_state = head_combiner(
-        present_rows,
-        prior_rows,
-        first_norm_gain,
-        token_shift_share,
-        receptance_weight,
-        key_weight,
-        value_weight,
-        decay_down_map,
-        decay_own,
-        decay_offset,
-        strength_down_map,
-        alpha_own,
-        removal_key_scale,
-        key_damping,
-        self_term_weight,
-        head_norm_gain,
-        state,
-    )
-    layer_out = tail(
-        mixed_inputs, tokens, second_norm_gain, routes, chosen_expert_weight,
+    return layer(
+        gather(pin(tokens), pin(previous)), first_norm_gain, token_shift_share, decay_offset,
+        removal_key_scale, key_damping, self_term_weight, head_norm_gain, second_norm_gain,
+        routes, chosen_expert_weight, receptance_weight, key_weight, value_weight,
+        decay_down_map, decay_up_map, strength_down_map, strength_up_map, state,
         output_weight, expert_gate_weight, expert_up_weight, expert_down_weight,
     )
-    return (layer_out, new_state)
 
 
 def solution(mesh):

time: 94.7 us -> 66.9 us (0.71)
  Pallas kernels: 51.1 us -> 63.5 us
  blocking collectives: 11 us -> 0 us
  local copies, waits for them, and re-layouts: 13.6 us -> 2.63 us
  matrix products: 10.2 us -> 0 us
  other arithmetic: 7.24 us -> 0 us
    pallas_call x1 -> x2, Pallas kernels: 51.1 us -> 63.5 us  [the longest x1 56.5 us: layer(): pl.pallas_call(layer_kernel, out_shape=(pltpu.VMEM((32, 512), BF16), pltp...]
    all_gather x1 -> x0, blocking collectives: 11 us -> none  [in_one_piece(): result = lax.all_gather(both, axis, axis=dim, tiled=True)]
    dot_general x7 -> x0, matrix products: 10.2 us -> none  [the longest x5 5.64 us: project(): return jnp.dot(inputs, weight, preferred_element_type=jnp.float32)]
    add x1 -> x0, other arithmetic: 4.56 us -> none  [head_combiner(): state * decay[:, :, None, :]]
    unnamed x25 -> x2, local copies, waits for them, and re-layouts: 6.63 us -> 2.63 us
    mul x5 -> x0, local copies, waits for them, and re-layouts: 3.04 us -> none  [the longest x1 1.34 us: head_combiner(): centered * lax.rsqrt(variance + GROUP_EPS)]
    reshape x6 -> x0, local copies, waits for them, and re-layouts: 2.01 us -> none  [the longest x1 0.92 us: tail(): by_choice.reshape(1, 128)]
    mul x2 -> x0, other arithmetic: 1.32 us -> none  [the longest x1 1.21 us: head_combiner(): jnp.sum(receptance_rows * blended_rows * self_term_weight, axis=-1, keepd...]
where the time goes in v2:
time: 66.9 us; the launch traced here: 66.7 us
  Pallas kernels  63.5 us (95%)
  local copies, waits for them, and re-layouts  2.63 us (4%)
    pallas_call x1, Pallas kernels, layer(): pl.pallas_call(layer_kernel, out_shape=(pltpu.VMEM((32, 512), BF16), pltp...  56.5 us
    pallas_call x1, Pallas kernels, gather(): pl.pallas_call(gather_kernel, out_shape=jax.ShapeDtypeStruct((N_TP, 64, 5...  7.01 us
    unnamed x2, local copies, waits for them, and re-layouts  2.63 us

profile of v2, /device:TPU:1, one launch (start us, length us, event | category | flops | bytes accessed | tf_op | source)
XLA Modules:
  0.0 66.7 jit_solution(14637907483714958977)
XLA Ops:
  0.6 7.0 %gather.1.rows_ref = bf16[4,64,512]{2,1,0:T(8,128)(2,1)S(1)} custom-call(bf16[32,512]{1,0:T(8,128)(2,1)} %tokens_hbm.1, bf16[32,512]{1,0:T(8,128)(2,1)} %previous_hbm.1), custom_call_target="tpu_custom_call" | custom-call | tf_op jit(solution)/shard_map/gather/pallas_call | solution.py:80
  7.7 56.5 %layer.1 = (bf16[32,512]{1,0:T(8,128)(2,1)S(1)}, f32[32,4,64,64]{3,2,1,0:T(8,128)S(1)}) custom-call(bf16[4,64,512]{2,1,0:T(8,128)(2,1)S(1)} %gather.1.rows_ref, f32[1,2048]{1,0:T(1,128)} %bitcast.8, f32[5,2048]{1,0:T(8,128)} %share_hbm.1, f32[1,256]{1,0:T(1,128)} %bitcast.12, f32[1,256]{1,0:T(1,128)} %bitcast.13, f32[1,256]{1,0:T(1,128)} %bitcast.14, ...), custom_call_target="tpu_custom_call" | custom-call | tf_op jit(solution)/shard_map/layer/pallas_call | solution.py:453
  64.1 0.6 copy.28
  64.7 2.0 %copy.29 = f32[32,4,64,64]{3,2,1,0:T(8,128)} copy(f32[32,4,64,64]{3,2,1,0:T(8,128)S(1)} %get-tuple-element.3) | data formatting | bytes 4194304

commit v3 on v2

--- a/solution.py
+++ b/solution.py
@@ -18,6 +18,7 @@
 GROUPS = 4
 NS = N_EP // GROUPS
 ORDER = (0, 3, 1, 2)
+EARLY = 15
 SLOTS = 3
 KEPT = 4 * SLOTS * NS
 PACKED = KEPT + NS
@@ -45,7 +46,12 @@
     return jnp.where(m == 12, 3, m + third(m))
 
 
-def gather_kernel(tokens_hbm, previous_hbm, rows_ref, load_sem, send_sem, recv_sem):
+def gather_kernel(
+    tokens_hbm, previous_hbm, *refs,
+):
+    kept = len(PARTS)
+    sources, (rows_ref, *targets) = refs[:kept], refs[kept : 2 * kept + 1]
+    load_sem, part_sem, send_sem, recv_sem = refs[2 * kept + 1 :]
     tp = lax.axis_index("tp")
     loads = [
         pltpu.make_async_copy(tokens_hbm, rows_ref.at[tp, pl.ds(0, 32)], load_sem.at[0]),
@@ -58,6 +64,13 @@
         pl.semaphore_signal(
             barrier, inc=1, device_id={"tp": lax.rem(tp + d, N_TP)}, device_id_type=MESH
         )
+    part_loads = []
+    for n, (source, target, (shape, dtype, cut)) in enumerate(zip(sources, targets, PARTS)):
+        if cut:
+            source = source.at[:, pl.ds(pl.multiple_of(tp * cut, cut), cut)]
+        load = pltpu.make_async_copy(source, target, part_sem.at[n])
+        load.start()
+        part_loads.append(load)
     for load in loads:
         load.wait()
     pl.semaphore_wait(barrier, N_TP - 1)
@@ -70,24 +83,51 @@
         )
         copy.start()
         copies.append(copy)
+    for load in part_loads:
+        load.wait()
     for copy in copies:
         copy.wait()
 
 
-def gather(tokens, previous):
+PARTS = [
+    ((1, 2048), F32, 0),
+    ((5, 2048), F32, 0),
+    ((1, 256), F32, 0),
+    ((1, 256), F32, 0),
+    ((1, 256), F32, 0),
+    ((4, 64), F32, 0),
+    ((1, 256), F32, 0),
+    ((1, 512), F32, 512),
+    ((4, 32), jnp.int32, 0),
+    ((4, 32), F32, 0),
+    ((2048, 128), BF16, 0),
+    ((2048, 128), BF16, 0),
+    ((2048, 256), BF16, 0),
+    ((2048, 256), BF16, 0),
+    ((2048, 256), BF16, 0),
+    ((128, 256), BF16, 256),
+    ((128, 256), BF16, 256),
+    ((32, 4, 64, 64), F32, 0),
+    ((256, 2048), BF16, 0),
+]
+
+
+def gather(tokens, previous, parts):
     hbm = pl.BlockSpec(memory_space=pltpu.HBM)
+    vmem = pl.BlockSpec(memory_space=pltpu.VMEM)
     dma = pltpu.SemaphoreType.DMA
     return pl.pallas_call(
         gather_kernel,
-        out_shape=jax.ShapeDtypeStruct((N_TP, 64, 512), BF16),
-        in_specs=[hbm, hbm],
-        out_specs=pl.BlockSpec(memory_space=pltpu.VMEM),
-        scratch_shapes=[dma((2,)), dma((N_TP - 1,)), dma((N_TP - 1,))],
+        out_shape=[pltpu.VMEM((N_TP, 64, 512), BF16)]
+        + [pltpu.VMEM(shape, dtype) for shape, dtype, _ in PARTS],
+        in_specs=[hbm] * (2 + len(PARTS)),
+        out_specs=[vmem] * (1 + len(PARTS)),
+        scratch_shapes=[dma((2,)), dma((len(PARTS),)), dma((N_TP - 1,)), dma((N_TP - 1,))],
         name="gather",
         compiler_params=pltpu.CompilerParams(
-            collective_id=0, has_side_effects=True, vmem_limit_bytes=4 * 1024 * 1024
+            collective_id=0, has_side_effects=True, vmem_limit_bytes=16 * 1024 * 1024
         ),
-    )(tokens, previous)
+    )(pin(tokens), pin(previous), *map(pin, parts))
 
 
 def head_sums(values):
@@ -104,51 +144,21 @@
 
 def layer_kernel(
     rows_ref,
-    gain_one_hbm, share_hbm, offset_hbm, key_scale_hbm, damping_hbm, self_hbm, head_gain_hbm,
-    gain_hbm, routes_hbm, weight_hbm,
-    wr_hbm, wk_hbm, wv_hbm, dd_hbm, du_hbm, sd_hbm, su_hbm, state_hbm,
-    wout_hbm, wg_hbm, wu_hbm, wd_hbm,
+    gain_one_ref, share_ref, offset_ref, key_scale_ref, damping_ref, self_pair, head_gain_ref,
+    gain_ref, routes_ref, weight_ref, dd, sd, wk, wr, wv, du, su, old_state, wout,
+    wg_hbm, wu_hbm, wd_hbm,
     out_ref, state,
-    gain_one_ref, share_ref, offset_ref, key_scale_ref, damping_ref, self_pair, head_gain_ref,
-    gain_ref, routes_ref, weight_ref, self_ref, routes_row_ref, routes_tiled_ref,
-    wr, wk, wv, dd, du, sd, su, along_scr, query_scr, rows_scr,
-    wout, wg, wu, wd, place, take, pick, unpick,
+    self_ref, routes_row_ref, routes_tiled_ref, along_scr, query_scr, rows_scr,
+    wg, wu, wd, place, take, pick, unpick,
     rs_send, rs_recv, residual, send_a, recv_a, gathered, down_send, down_recv, send_b, recv_b,
-    w_sem, h_sem, p_sem, rs_ssem, rs_rsem, a_ssem, a_rsem, g_ssem, g_rsem, d_ssem, d_rsem, b_ssem, b_rsem,
+    w_sem, rs_ssem, rs_rsem, a_ssem, a_rsem, g_ssem, g_rsem, d_ssem, d_rsem, b_ssem, b_rsem,
 ):
     me = lax.axis_index("ep")
     tp = lax.axis_index("tp")
-    own = pl.ds(pl.multiple_of(tp * 256, 256), 256)
-    small_loads = [
-        pltpu.make_async_copy(source, target, p_sem.at[n])
-        for n, (source, target) in enumerate(
-            [
-                (gain_one_hbm, gain_one_ref), (share_hbm, share_ref), (offset_hbm, offset_ref),
-                (key_scale_hbm, key_scale_ref), (damping_hbm, damping_ref), (self_hbm, self_pair),
-                (head_gain_hbm, head_gain_ref),
-                (gain_hbm.at[:, pl.ds(pl.multiple_of(tp * 512, 512), 512)], gain_ref),
-                (routes_hbm, routes_ref), (weight_hbm, weight_ref),
-            ]
-        )
-    ]
-    for load in small_loads:
-        load.start()
-    head_loads = [
-        pltpu.make_async_copy(source, target, h_sem.at[n])
-        for n, (source, target) in enumerate(
-            [
-                (dd_hbm, dd), (sd_hbm, sd), (wk_hbm, wk), (wr_hbm, wr), (wv_hbm, wv),
-                (du_hbm.at[:, own], du), (su_hbm.at[:, own], su), (state_hbm, state),
-            ]
-        )
-    ]
-    for load in head_loads:
-        load.start()
     loads = [
-        pltpu.make_async_copy(wout_hbm, wout, w_sem.at[0]),
-        pltpu.make_async_copy(wg_hbm.at[0], wg, w_sem.at[1]),
-        pltpu.make_async_copy(wu_hbm.at[0], wu, w_sem.at[2]),
-        pltpu.make_async_copy(wd_hbm.at[0], wd, w_sem.at[3]),
+        pltpu.make_async_copy(wg_hbm.at[0], wg, w_sem.at[0]),
+        pltpu.make_async_copy(wu_hbm.at[0], wu, w_sem.at[1]),
+        pltpu.make_async_copy(wd_hbm.at[0], wd, w_sem.at[2]),
     ]
     for load in loads:
         load.start()
@@ -166,8 +176,6 @@
 
     lax.fori_loop(1, N_EP, greet, 0)
 
-    for load in small_loads:
-        load.wait()
     for h in range(4):
         self_ref[:, h * 64 : (h + 1) * 64] = self_pair[h : h + 1, :]
     for c in range(4):
@@ -185,16 +193,12 @@
         normed = rows_ref[t, 0:32, :].astype(F32) * scale * gain_one_ref[:, span]
         change = rows_ref[t, 32:64, :].astype(F32) - normed
         for n, (m, weight) in enumerate([(3, dd), (4, sd), (1, wk), (0, wr), (2, wv)]):
-            if t == 0:
-                head_loads[n].wait()
             shifted = (normed + change * share_ref[m : m + 1, span]).astype(BF16)
             term = dot(shifted, weight[span, :])
             sums[n] = term if t == 0 else sums[n] + term
     low, strength_low, key, receptance, value = sums
-    head_loads[5].wait()
     decay = dot(jnp.tanh(low).astype(BF16), du[...]) + offset_ref[...]
     decay = jnp.exp(jax.nn.sigmoid(decay) * -(2.718281828459045 ** -0.5))
-    head_loads[6].wait()
     alpha = jax.nn.sigmoid(dot(strength_low.astype(BF16), su[...]))
     removal = key * key_scale_ref[...]
     removal = removal * lax.rsqrt(head_sums(removal * removal) + KEY_EPS)
@@ -206,12 +210,11 @@
             [strong * receptance, blended * receptance, blended * receptance * self_ref[...]], axis=0
         )
     )
-    head_loads[7].wait()
     for h in range(4):
         lanes = slice(h * 64, (h + 1) * 64)
         asked = jnp.concatenate([removal[:, lanes], query[:, lanes]], axis=0).astype(BF16)
         for q in range(8):
-            held = state[4 * q : 4 * q + 4, h].reshape(256, 64).astype(BF16)
+            held = old_state[4 * q : 4 * q + 4, h].reshape(256, 64).astype(BF16)
             answer = lax.dot_general(
                 asked, held, (((1,), (1,)), ((), ())), preferred_element_type=F32
             )
@@ -230,7 +233,6 @@
         for h in range(4):
             rows_scr[n, h] = values[:, h * 64 : (h + 1) * 64]
 
-    loads[0].wait()
     for j in range(N_TP):
         rs_send[j] = dot(mixed, wout[:, j * 512 : (j + 1) * 512]).astype(BF16)
     pl.semaphore_wait(barrier, N_EP - 1 + N_TP - 1)
@@ -346,10 +348,10 @@
                 left, right, (((0,), (0,)), ((), ())),
                 preferred_element_type=F32, precision=lax.Precision.HIGHEST,
             )
-            state[s, h] = state[s, h] * decay_row + change
+            state[s, h] = old_state[s, h] * decay_row + change
         return carry
 
-    lax.fori_loop(0, 32, renew, 0)
+    lax.fori_loop(0, EARLY, renew, 0)
 
     def wait_bytes(ref, sem):
         pltpu.make_async_copy(ref, ref, sem).wait()
@@ -369,7 +371,7 @@
             )
             copy.start()
             g_copies.append(copy)
-    for load in loads[1:]:
+    for load in loads:
         load.wait()
     d_copies = []
     for n, group in enumerate(ORDER):
@@ -429,6 +431,7 @@
 
         lax.fori_loop(max(1, first), first + NS, send_back, 0)
     recv_b[me] = send_b[0]
+    lax.fori_loop(EARLY, 32, renew, 0)
     some = pl.ds(0, N_EP - 1)
     wait_bytes(recv_b.at[some], b_rsem)
     result = dot(take[...], recv_b[...].reshape(N_EP * 16, 128))
@@ -443,10 +446,7 @@
     wait_bytes(send_b.at[some], b_ssem)
 
 
-def layer(
-    rows, gain_one, share, offset, key_scale, damping, self_weight, head_gain, gain, routes, weight,
-    wr, wk, wv, dd, du, sd, su, state, wout, wg, wu, wd,
-):
+def layer(gathered, wg, wu, wd):
     vmem = pl.BlockSpec(memory_space=pltpu.VMEM)
     hbm = pl.BlockSpec(memory_space=pltpu.HBM)
     dma = pltpu.SemaphoreType.DMA
@@ -456,33 +456,15 @@
             pltpu.VMEM((32, 512), BF16),
             pltpu.VMEM((32, 4, 64, 64), F32),
         ),
-        in_specs=[vmem] + [hbm] * 22,
+        in_specs=[vmem] * 20 + [hbm] * 3,
         out_specs=(vmem, vmem),
         scratch_shapes=[
-            pltpu.VMEM((1, 2048), F32),
-            pltpu.VMEM((5, 2048), F32),
-            pltpu.VMEM((1, 256), F32),
-            pltpu.VMEM((1, 256), F32),
-            pltpu.VMEM((1, 256), F32),
-            pltpu.VMEM((4, 64), F32),
-            pltpu.VMEM((1, 256), F32),
-            pltpu.VMEM((1, 512), F32),
-            pltpu.VMEM((4, 32), jnp.int32),
-            pltpu.VMEM((4, 32), F32),
             pltpu.VMEM((1, 256), F32),
             pltpu.VMEM((1, 128), jnp.int32),
             pltpu.VMEM((4, 256), jnp.int32),
-            pltpu.VMEM((2048, 256), BF16),
-            pltpu.VMEM((2048, 256), BF16),
-            pltpu.VMEM((2048, 256), BF16),
-            pltpu.VMEM((2048, 128), BF16),
-            pltpu.VMEM((128, 256), BF16),
-            pltpu.VMEM((2048, 128), BF16),
-            pltpu.VMEM((128, 256), BF16),
             pltpu.VMEM((32, 256), F32),
             pltpu.VMEM((32, 256), F32),
             pltpu.VMEM((5, 4, 32, 64), F32),
-            pltpu.VMEM((256, 2048), BF16),
             pltpu.VMEM((2048, 256), BF16),
             pltpu.VMEM((2048, 256), BF16),
             pltpu.VMEM((256, 2048), BF16),
@@ -500,9 +482,7 @@
             pltpu.VMEM((GROUPS, N_TP - 1, KEPT, 128), BF16),
             pltpu.VMEM((N_EP, 16, 128), BF16),
             pltpu.VMEM((N_EP, 16, 128), BF16),
-            dma((4,)),
-            dma((8,)),
-            dma((10,)),
+            dma((3,)),
             dma((N_TP - 1,)),
             dma((N_TP - 1,)),
             dma,
@@ -516,13 +496,9 @@
         ],
         name="layer",
         compiler_params=pltpu.CompilerParams(
-            collective_id=1, has_side_effects=True, vmem_limit_bytes=48 * 1024 * 1024
+            collective_id=1, has_side_effects=True, vmem_limit_bytes=24 * 1024 * 1024
         ),
-    )(
-        rows, *map(pin, (gain_one.reshape(1, 2048), share, offset.reshape(1, 256), key_scale.reshape(1, 256),
-        damping.reshape(1, 256), self_weight, head_gain.reshape(1, 256),
-        gain.reshape(1, 2048), routes.T, weight.T, wr, wk, wv, dd, du, sd, su, state, wout, wg, wu, wd))
-    )
+    )(*gathered, pin(wg), pin(wu), pin(wd))
 
 
 def shards(
@@ -551,13 +527,17 @@
     expert_up_weight,
     expert_down_weight,
 ):
-    return layer(
-        gather(pin(tokens), pin(previous)), first_norm_gain, token_shift_share, decay_offset,
-        removal_key_scale, key_damping, self_term_weight, head_norm_gain, second_norm_gain,
-        routes, chosen_expert_weight, receptance_weight, key_weight, value_weight,
-        decay_down_map, decay_up_map, strength_down_map, strength_up_map, state,
-        output_weight, expert_gate_weight, expert_up_weight, expert_down_weight,
+    gathered = gather(
+        tokens, previous,
+        [
+            first_norm_gain.reshape(1, 2048), token_shift_share, decay_offset.reshape(1, 256),
+            removal_key_scale.reshape(1, 256), key_damping.reshape(1, 256), self_term_weight,
+            head_norm_gain.reshape(1, 256), second_norm_gain.reshape(1, 2048), routes.T,
+            chosen_expert_weight.T, decay_down_map, strength_down_map, key_weight,
+            receptance_weight, value_weight, decay_up_map, strength_up_map, state, output_weight,
+        ],
     )
+    return layer(gathered, expert_gate_weight, expert_up_weight, expert_down_weight)
 
 
 def solution(mesh):

time: 66.9 us -> 60.4 us (0.903)
  Pallas kernels: 63.5 us -> 57.1 us
    pallas_call x1, Pallas kernels: 56.5 us -> 49.8 us  [layer(): pl.pallas_call(layer_kernel, out_shape=(pltpu.VMEM((32, 512), BF16), pltp...]
where the time goes in v3:
time: 60.4 us
  Pallas kernels  57.1 us (95%)
  local copies, waits for them, and re-layouts  2.63 us (4%)
  between operations  0.66 us (1%)
    pallas_call x1, Pallas kernels, layer(): pl.pallas_call(layer_kernel, out_shape=(pltpu.VMEM((32, 512), BF16), pltp...  49.8 us
    pallas_call x1, Pallas kernels, gather(): pl.pallas_call(gather_kernel, out_shape=[pltpu.VMEM((N_TP, 64, 512), BF16...  7.23 us
    unnamed x2, local copies, waits for them, and re-layouts  2.63 us

profile of v3, /device:TPU:1, one launch (start us, length us, event | category | flops | bytes accessed | tf_op | source)
XLA Modules:
  0.0 60.4 jit_solution(3917251465254336037)
XLA Ops:
  0.6 7.2 %gather.1 = (bf16[4,64,512]{2,1,0:T(8,128)(2,1)S(1)}, f32[1,2048]{1,0:T(1,128)S(1)}, f32[5,2048]{1,0:T(8,128)S(1)}, f32[1,256]{1,0:T(1,128)S(1)}, f32[1,256]{1,0...) custom-call(bf16[32,512]{1,0:T(8,128)(2,1)} %tokens_hbm.1, ...), custom_call_target="tpu_custom_call" | custom-call | tf_op jit(solution)/shard_map/gather/pallas_call | solution.py:119
  7.9 49.8 %layer.1 = (bf16[32,512]{1,0:T(8,128)(2,1)S(1)}, f32[32,4,64,64]{3,2,1,0:T(8,128)S(1)}) custom-call(bf16[4,64,512]{2,1,0:T(8,128)(2,1)S(1)} %get-tuple-element.22.rows_ref, f32[1,2048]{1,0:T(1,128)S(1)} %get-tuple-element.23.gain_one_ref, f32[5,2048]{1,0:T(8,128)S(1)} %get-tuple-element.24.share_ref, f32[1,256]{1,0:T(1,128)S(1)} %get-tuple-element.25.offset_ref, ...), custom_call_target="tpu_custom_call" | custom-call | tf_op jit(solution)/shard_map/layer/pallas_call | solution.py:453
  57.7 0.6 %copy.28 = bf16[32,512]{1,0:T(8,128)(2,1)} copy(bf16[32,512]{1,0:T(8,128)(2,1)S(1)} %get-tuple-element.42) | data formatting | bytes 65536
  58.3 2.0 %copy.29 = f32[32,4,64,64]{3,2,1,0:T(8,128)} copy(f32[32,4,64,64]{3,2,1,0:T(8,128)S(1)} %get-tuple-element.43) | data formatting | bytes 4194304

commit v4 on v3

--- a/solution.py
+++ b/solution.py
@@ -18,10 +18,12 @@
 GROUPS = 4
 NS = N_EP // GROUPS
 ORDER = (0, 3, 1, 2)
+RELAYED = (0, 1, 1, 1)
 EARLY = 15
 SLOTS = 3
 KEPT = 4 * SLOTS * NS
 PACKED = KEPT + NS
+CUT = 104
 F32 = jnp.float32
 BF16 = jnp.bfloat16
 
@@ -356,27 +358,50 @@
     def wait_bytes(ref, sem):
         pltpu.make_async_copy(ref, ref, sem).wait()
 
-    g_copies = []
-    for n, group in enumerate(ORDER):
-        first = group * NS
-        count = NS - 1 if group == 0 else NS
-        wait_bytes(recv_a.at[pl.ds(first, count)], a_rsem.at[group])
+    ahead, behind = lax.rem(tp + 1, N_TP), lax.rem(tp + 3, N_TP)
+    across = lax.rem(tp + 2, N_TP)
+    sent = []
+
+    def send(peer, source, target, send_sem, recv_sem):
+        copy = pltpu.make_async_remote_copy(
+            src_ref=source, dst_ref=target, send_sem=send_sem, recv_sem=recv_sem,
+            device_id={"tp": peer}, device_id_type=MESH,
+        )
+        copy.start()
+        sent.append(copy)
+        return copy
+
+    own_up, own_down, far_up, far_down = {}, {}, {}, {}
+
+    def collect(n):
+        first = ORDER[n] * NS
+        count = NS - 1 if ORDER[n] == 0 else NS
+        wait_bytes(recv_a.at[pl.ds(first, count)], a_rsem.at[ORDER[n]])
         tiles = recv_a[first : first + NS].reshape(NS * 16, 128)
         gathered[n, tp] = dot(pick[...], tiles).astype(BF16)
-        for d in (2, 1, 3):
-            copy = pltpu.make_async_remote_copy(
-                src_ref=gathered.at[n, tp], dst_ref=gathered.at[n, tp],
-                send_sem=g_ssem.at[n, d - 1], recv_sem=g_rsem.at[n, d - 1],
-                device_id={"tp": lax.rem(tp + d, N_TP)}, device_id_type=MESH,
-            )
-            copy.start()
-            g_copies.append(copy)
-    for load in loads:
-        load.wait()
-    d_copies = []
-    for n, group in enumerate(ORDER):
-        for copy in g_copies[3 * n : 3 * n + 3]:
-            copy.wait_recv()
+        mine = gathered.at[n, tp]
+        own_up[n] = send(ahead, mine, mine, g_ssem.at[n, 0], g_rsem.at[n, 0])
+        own_down[n] = send(behind, mine, mine, g_ssem.at[n, 1], g_rsem.at[n, 1])
+        if not RELAYED[n]:
+            far_up[n] = send(across, mine, mine, g_ssem.at[n, 2], g_rsem.at[n, 2])
+
+    def pass_on(n):
+        own_up[n].wait_recv()
+        part = gathered.at[n, behind, pl.ds(0, CUT)]
+        far_up[n] = send(ahead, part, part, g_ssem.at[n, 2], g_rsem.at[n, 2])
+        own_down[n].wait_recv()
+        part = gathered.at[n, ahead, pl.ds(CUT, PACKED - CUT)]
+        far_down[n] = send(behind, part, part, g_ssem.at[n, 3], g_rsem.at[n, 3])
+
+    arriving = {}
+
+    def experts(n):
+        far_up[n].wait_recv()
+        if RELAYED[n]:
+            far_down[n].wait_recv()
+        else:
+            own_up[n].wait_recv()
+            own_down[n].wait_recv()
         rows, sums = [], None
         for t in range(N_TP):
             for k in range(4):
@@ -397,15 +422,12 @@
                 down_send[n, j, k * 3 * NS : (k + 1) * 3 * NS, :] = terms[
                     :, k * 128 : (k + 1) * 128
                 ]
-        for d in (2, 1, 3):
-            peer = lax.rem(tp + d, N_TP)
-            copy = pltpu.make_async_remote_copy(
-                src_ref=down_send.at[n, peer], dst_ref=down_recv.at[n, d - 1],
-                send_sem=d_ssem.at[n, d - 1], recv_sem=d_rsem.at[n, d - 1],
-                device_id={"tp": peer}, device_id_type=MESH,
+        for peer, slot in ((across, 2), (ahead, 0), (behind, 1)):
+            copy = send(
+                peer, down_send.at[n, peer], down_recv.at[n, slot],
+                d_ssem.at[n, slot], d_rsem.at[n, slot],
             )
-            copy.start()
-            d_copies.append(copy)
+            arriving.setdefault(n, []).append(copy)
 
     def back_copy(r):
         return pltpu.make_async_remote_copy(
@@ -414,22 +436,39 @@
             device_id={"ep": lax.rem(me + r, N_EP)}, device_id_type=MESH,
         )
 
-    for n, group in enumerate(ORDER):
-        for copy in d_copies[3 * n : 3 * n + 3]:
+    def send_back(r, carry):
+        back_copy(r).start()
+        return carry
+
+    def give_back(n):
+        for copy in arriving[n]:
             copy.wait_recv()
         total = down_send[n, tp].astype(F32)
-        for d in range(N_TP - 1):
+        for d in range(len(arriving[n])):
             total = total + down_recv[n, d].astype(F32)
-        first = group * NS
+        first = ORDER[n] * NS
         send_b[first : first + NS] = (
             dot(unpick[...], total.astype(BF16)).astype(BF16).reshape(NS, 16, 128)
         )
-
-        def send_back(r, carry):
-            back_copy(r).start()
-            return carry
-
         lax.fori_loop(max(1, first), first + NS, send_back, 0)
+
+    collect(0)
+    collect(1)
+    collect(2)
+    collect(3)
+    for load in loads:
+        load.wait()
+    experts(0)
+    pass_on(1)
+    pass_on(2)
+    pass_on(3)
+    experts(1)
+    experts(2)
+    experts(3)
+    give_back(0)
+    give_back(1)
+    give_back(2)
+    give_back(3)
     recv_b[me] = send_b[0]
     lax.fori_loop(EARLY, 32, renew, 0)
     some = pl.ds(0, N_EP - 1)
@@ -440,7 +479,7 @@
         out_ref[:, k * 128 : (k + 1) * 128] = (
             residual[:, k * 128 : (k + 1) * 128] + part
         ).astype(BF16)
-    for copy in g_copies + d_copies:
+    for copy in sent:
         copy.wait_send()
     wait_bytes(send_a.at[some], a_ssem)
     wait_bytes(send_b.at[some], b_ssem)
@@ -479,7 +518,7 @@
             pltpu.VMEM((N_EP, 16, 128), BF16),
             pltpu.VMEM((GROUPS, N_TP, PACKED, 128), BF16),
             pltpu.VMEM((GROUPS, N_TP, KEPT, 128), BF16),
-            pltpu.VMEM((GROUPS, N_TP - 1, KEPT, 128), BF16),
+            pltpu.VMEM((GROUPS, 3, KEPT, 128), BF16),
             pltpu.VMEM((N_EP, 16, 128), BF16),
             pltpu.VMEM((N_EP, 16, 128), BF16),
             dma((3,)),
@@ -487,10 +526,10 @@
             dma((N_TP - 1,)),
             dma,
             dma((GROUPS,)),
-            dma((GROUPS, N_TP - 1)),
-            dma((GROUPS, N_TP - 1)),
-            dma((GROUPS, N_TP - 1)),
-            dma((GROUPS, N_TP - 1)),
+            dma((GROUPS, 4)),
+            dma((GROUPS, 4)),
+            dma((GROUPS, 4)),
+            dma((GROUPS, 4)),
             dma,
             dma,
         ],
@@ -499,6 +538,36 @@
             collective_id=1, has_side_effects=True, vmem_limit_bytes=24 * 1024 * 1024
         ),
     )(*gathered, pin(wg), pin(wu), pin(wd))
+
+
+def store_kernel(out_ref, state_ref, out_hbm, state_hbm, sem):
+    copies = [pltpu.make_async_copy(out_ref, out_hbm, sem.at[0])]
+    for n in range(4):
+        some = pl.ds(n * 8, 8)
+        copies.append(
+            pltpu.make_async_copy(state_ref.at[some], state_hbm.at[some], sem.at[1 + n])
+        )
+    for copy in copies:
+        copy.start()
+    for copy in copies:
+        copy.wait()
+
+
+def store(out, state):
+    vmem = pl.BlockSpec(memory_space=pltpu.VMEM)
+    hbm = pl.BlockSpec(memory_space=pl.ANY)
+    return pl.pallas_call(
+        store_kernel,
+        out_shape=(
+            jax.ShapeDtypeStruct(out.shape, out.dtype),
+            jax.ShapeDtypeStruct(state.shape, state.dtype),
+        ),
+        in_specs=[vmem, vmem],
+        out_specs=(hbm, hbm),
+        scratch_shapes=[pltpu.SemaphoreType.DMA((5,))],
+        name="store",
+        compiler_params=pltpu.CompilerParams(vmem_limit_bytes=8 * 1024 * 1024),
+    )(out, state)
 
 
 def shards(
@@ -537,7 +606,7 @@
             receptance_weight, value_weight, decay_up_map, strength_up_map, state, output_weight,
         ],
     )
-    return layer(gathered, expert_gate_weight, expert_up_weight, expert_down_weight)
+    return store(*layer(gathered, expert_gate_weight, expert_up_weight, expert_down_weight))
 
 
 def solution(mesh):

time: 60.4 us -> 58.9 us (0.975)
  local copies, waits for them, and re-layouts: 2.63 us -> 0 us
  Pallas kernels: 57.1 us -> 58.1 us
    unnamed x2 -> x0, local copies, waits for them, and re-layouts: 2.63 us -> none
    pallas_call x0 -> x1, Pallas kernels: none -> 2.06 us  [store(): pl.pallas_call(store_kernel, out_shape=(jax.ShapeDtypeStruct(out.shape, o...]
    pallas_call x1, Pallas kernels: 49.8 us -> 48.8 us  [layer(): pl.pallas_call(layer_kernel, out_shape=(pltpu.VMEM((32, 512), BF16), pltp...]
where the time goes in v4:
time: 58.9 us; the launch traced here: 58.8 us
  Pallas kernels  58.1 us (99%)
  between operations  0.66 us (1%)
    pallas_call x1, Pallas kernels, layer(): pl.pallas_call(layer_kernel, out_shape=(pltpu.VMEM((32, 512), BF16), pltp...  48.8 us
    pallas_call x1, Pallas kernels, gather(): pl.pallas_call(gather_kernel, out_shape=[pltpu.VMEM((N_TP, 64, 512), BF16...  7.23 us
    pallas_call x1, Pallas kernels, store(): pl.pallas_call(store_kernel, out_shape=(jax.ShapeDtypeStruct(out.shape, o...  2.06 us

profile of v4, /device:TPU:1, one launch (start us, length us, event | category | flops | bytes accessed | tf_op | source)
XLA Modules:
  0.0 58.8 jit_solution(17284679243838770401)
XLA Ops:
  0.6 7.2 %gather.1 = (bf16[4,64,512]{2,1,0:T(8,128)(2,1)S(1)}, f32[1,2048]{1,0:T(1,128)S(1)}, f32[5,2048]{1,0:T(8,128)S(1)}, f32[1,256]{1,0:T(1,128)S(1)}, f32[1,256]{1,0...) custom-call(bf16[32,512]{1,0:T(8,128)(2,1)} %tokens_hbm.1, ...), custom_call_target="tpu_custom_call" | custom-call | tf_op jit(solution)/shard_map/gather/pallas_call | solution.py:121
  7.9 48.8 %layer.1 = (bf16[32,512]{1,0:T(8,128)(2,1)S(1)}, f32[32,4,64,64]{3,2,1,0:T(8,128)S(1)}) custom-call(bf16[4,64,512]{2,1,0:T(8,128)(2,1)S(1)} %get-tuple-element.24.rows_ref, f32[1,2048]{1,0:T(1,128)S(1)} %get-tuple-element.25.gain_one_ref, f32[5,2048]{1,0:T(8,128)S(1)} %get-tuple-element.26.share_ref, f32[1,256]{1,0:T(1,128)S(1)} %get-tuple-element.27.offset_ref, ...), custom_call_target="tpu_custom_call" | custom-call | tf_op jit(solution)/shard_map/layer/pallas_call | solution.py:492
  56.7 2.1 %store.1 = (bf16[32,512]{1,0:T(8,128)(2,1)}, f32[32,4,64,64]{3,2,1,0:T(8,128)}) custom-call(bf16[32,512]{1,0:T(8,128)(2,1)S(1)} %get-tuple-element.44.out_ref, f32[32,4,64,64]{3,2,1,0:T(8,128)S(1)} %get-tuple-element.45.state_ref), custom_call_target="tpu_custom_call" | custom-call | tf_op jit(solution)/shard_map/store/pallas_call | solution.py:559

commit v5 on v4

--- a/solution.py
+++ b/solution.py
@@ -176,7 +176,10 @@
         )
         return carry
 
-    lax.fori_loop(1, N_EP, greet, 0)
+    lax.fori_loop(20, 44, greet, 0, unroll=4)
+    lax.fori_loop(4, 20, greet, 0, unroll=4)
+    lax.fori_loop(44, N_EP, greet, 0, unroll=4)
+    lax.fori_loop(1, 4, greet, 0)
 
     for h in range(4):
         self_ref[:, h * 64 : (h + 1) * 64] = self_pair[h : h + 1, :]
@@ -313,7 +316,7 @@
             out_copy(r, group).start()
             return carry
 
-        lax.fori_loop(max(1, group * NS), (group + 1) * NS, send_out, 0)
+        lax.fori_loop(max(1, group * NS), (group + 1) * NS, send_out, 0, unroll=5 if group == 0 else 4)
     recv_a[0] = send_a[me]
 
     seq_col = iota((32, 128), 0)
@@ -450,7 +453,7 @@
         send_b[first : first + NS] = (
             dot(unpick[...], total.astype(BF16)).astype(BF16).reshape(NS, 16, 128)
         )
-        lax.fori_loop(max(1, first), first + NS, send_back, 0)
+        lax.fori_loop(max(1, first), first + NS, send_back, 0, unroll=4 if first else 5)
 
     collect(0)
     collect(1)

time: 58.9 us -> 58.5 us (level)
  no operation moved by 1% of the time
where the time goes in v5:
time: 58.5 us; the launch traced here: 58.4 us
  Pallas kernels  57.7 us (99%)
  between operations  0.66 us (1%)
    pallas_call x1, Pallas kernels, layer(): pl.pallas_call(layer_kernel, out_shape=(pltpu.VMEM((32, 512), BF16), pltp...  48.5 us
    pallas_call x1, Pallas kernels, gather(): pl.pallas_call(gather_kernel, out_shape=[pltpu.VMEM((N_TP, 64, 512), BF16...  7.23 us
    pallas_call x1, Pallas kernels, store(): pl.pallas_call(store_kernel, out_shape=(jax.ShapeDtypeStruct(out.shape, o...  2.06 us

profile of v5, /device:TPU:1, one launch (start us, length us, event | category | flops | bytes accessed | tf_op | source)
XLA Modules:
  0.0 58.4 jit_solution(13369381958988510536)
XLA Ops:
  0.6 7.2 %gather.1 = (bf16[4,64,512]{2,1,0:T(8,128)(2,1)S(1)}, f32[1,2048]{1,0:T(1,128)S(1)}, f32[5,2048]{1,0:T(8,128)S(1)}, f32[1,256]{1,0:T(1,128)S(1)}, f32[1,256]{1,0...) custom-call(bf16[32,512]{1,0:T(8,128)(2,1)} %tokens_hbm.1, ...), custom_call_target="tpu_custom_call" | custom-call | tf_op jit(solution)/shard_map/gather/pallas_call | solution.py:121
  7.9 48.5 %layer.1 = (bf16[32,512]{1,0:T(8,128)(2,1)S(1)}, f32[32,4,64,64]{3,2,1,0:T(8,128)S(1)}) custom-call(bf16[4,64,512]{2,1,0:T(8,128)(2,1)S(1)} %get-tuple-element.24.rows_ref, f32[1,2048]{1,0:T(1,128)S(1)} %get-tuple-element.25.gain_one_ref, f32[5,2048]{1,0:T(8,128)S(1)} %get-tuple-element.26.share_ref, f32[1,256]{1,0:T(1,128)S(1)} %get-tuple-element.27.offset_ref, ...), custom_call_target="tpu_custom_call" | custom-call | tf_op jit(solution)/shard_map/layer/pallas_call | solution.py:495
  56.3 2.1 %store.1 = (bf16[32,512]{1,0:T(8,128)(2,1)}, f32[32,4,64,64]{3,2,1,0:T(8,128)}) custom-call(bf16[32,512]{1,0:T(8,128)(2,1)S(1)} %get-tuple-element.44.out_ref, f32[32,4,64,64]{3,2,1,0:T(8,128)S(1)} %get-tuple-element.45.state_ref), custom_call_target="tpu_custom_call" | custom-call | tf_op jit(solution)/shard_map/store/pallas_call | solution.py:562
